TPU v7x, 128 devices: a whole 4x4x4 slice. The times are simulated.
128 devices in a mesh: sp: 16 (over z, x), tp: 8 (over y, core).
Axes of the slice: x: 4, y: 4, z: 4, core: 2. Of those that a mesh axis runs over, the one named last changes fastest.
Arguments:
- resid: bfloat16 [12288, 3072], P('sp', 'tp'), may hold values from -12 to 12
- query: bfloat16 [12288, 1536], P('sp', 'tp'), may hold values from -6 to 6
- keys: bfloat16 [12288, 1536], P('sp', 'tp'), may hold values from -6 to 6
- values: bfloat16 [12288, 1536], P('sp', 'tp'), may hold values from -6 to 6
- out_gate: bfloat16 [12288, 1536], P('sp', 'tp'), may hold values from -6 to 6
- in_gate: float32 [16, 12288], P('tp', 'sp'), may hold values from -6 to 110
- forget: float32 [16, 12288], P('tp', 'sp'), may hold values from -1 to 16
- doc_ids: int32 [12288], P('sp'), may hold values from 0 to 7, never falling along the last dimension, each value on 1 to 3072 neighbouring positions
- head_gain: float32 [1536], P('tp'), may hold values from 0.1 to 1.9
- w_out: bfloat16 [1536, 3072], P('tp'), may hold values from -0.15625 to 0.15625
- ffn_gain: float32 [3072], replicated, may hold values from 0.1 to 1.9
- w_gate: bfloat16 [3072, 8448], P('sp', 'tp'), may hold values from -0.109375 to 0.109375
- w_value: bfloat16 [3072, 8448], P('sp', 'tp'), may hold values from -0.109375 to 0.109375
- conv_taps: float32 [3, 8448], P(None, 'tp'), may hold values from -3.5 to 3.5
- w_down: bfloat16 [8448, 3072], P('tp', 'sp'), may hold values from -0.0625 to 0.0625
Outputs:
- layer_out: bfloat16 [12288, 3072], P('sp', 'tp')
Inputs may be any that keep to these rules, and one draw needn't show every extreme that they name: `doc_ids`: document numbers never fall along the positions; each document is 1 to 3072 positions long.
All inputs are finite; a program needn't handle non-finite values.
Results may differ from a plain program's by a relative error of at most 0.02.
Values may be sent and summed in bfloat16 or wider, within the bound.
A program may use at most 128 MiB of HBM per device.

v0:
```python
import heapq

import jax
import jax.numpy as jnp
from jax import lax
from jax.experimental import pallas as pl
from jax.experimental.pallas import tpu as pltpu
from jax.sharding import PartitionSpec as P

DH = 96
ABSENT = -1e30
EPSILON = 1e-06
HEAD_FLOOR = 1.0
TOKENS = 768
WIDTH = 3072
ROWS = 192
OWN = 384
HEADS = 192
MAIN = 1024
CHUNK = 256
CHUNKS = TOKENS // CHUNK
UNIT = 48
BF = jnp.bfloat16
F32 = jnp.float32
MESH = pl.DeviceIdType.MESH
NT = (((1,), (1,)), ((), ()))
TN = (((0,), (0,)), ((), ()))

RATES = {"up": 4.6, "down": 2.2}
HOP = 2.2
DOWN_START = 42.0


def gather_plan():
    free = {}
    queue = []
    count = 0
    events = []

    def arrival(piece, axis, direction):
        tensor, colour, half, first, second = piece
        if (axis == "x") == (colour == 0):
            return (tensor, colour, half, (first + direction) % 4, second)
        return (tensor, colour, half, first, (second + direction) % 4)

    def enqueue(time, start):
        nonlocal count
        piece, axis, direction = start
        begin = max(time, free.get((axis, direction), 0.0))
        end = begin + RATES[piece[0]]
        free[(axis, direction)] = end
        count += 1
        heapq.heappush(queue, (end + HOP, count, arrival(piece, axis, direction)))

    def axes(colour):
        return ("x", "z") if colour == 0 else ("z", "x")

    def own(tensor):
        starts = []
        for which in (0, 1):
            for half in (0, 1):
                for colour in (0, 1):
                    axis = axes(colour)[which]
                    ahead = 1 if half == 0 else -1
                    for direction in (ahead, -ahead):
                        starts.append(((tensor, colour, half, 0, 0), axis, direction))
        return starts

    def follow(piece):
        tensor, colour, half, first, second = piece
        ahead = 1 if half == 0 else -1
        one, two = axes(colour)
        starts = []
        if second == 0:
            if first == ahead % 4:
                starts.append((piece, one, ahead))
            starts += [(piece, two, ahead), (piece, two, -ahead)]
        elif second == ahead % 4:
            starts.append((piece, two, ahead))
        return starts

    first_starts = own("up")
    for start in first_starts:
        enqueue(0.0, start)
    down_starts = own("down")
    pending = True
    while queue or pending:
        if pending and (not queue or queue[0][0] >= DOWN_START):
            pending = False
            events.append((DOWN_START, None, down_starts))
            for start in down_starts:
                enqueue(DOWN_START, start)
            continue
        time, _, piece = heapq.heappop(queue)
        starts = follow(piece)
        for start in starts:
            enqueue(time, start)
        events.append((time, piece, starts))
    return first_starts, events


def layer_kernel(
    resid, query, keys, values, out_gate, cols, rows, head_gain, w_out, own_gain, full_gain,
    w_up, w_down, taps, tap_tail,
    out,
    up, down, normed, share, sib, comb, near_l, near_r, far_l, far_r, residual,
    gate, value, gate_tail, value_tail, hidden, hidden_tail, edge, edge_tail, edge_out, edge_tail_out,
    scale, state_out, meta_out, states, metas,
    dshare, dsib, dcomb, dnear_l, dnear_r, dfar_l, dfar_r,
    send_up, recv_up, send_down, recv_down, local_sem,
    state_send, state_recv, meta_send, meta_recv, edge_send, edge_recv,
    sib_send, sib_recv, rs_send, rs_recv, ag_send, ag_recv, pass_send, pass_recv,
    dsib_send, dsib_recv, drs_send, drs_recv,
):
    s = lax.axis_index("sp")
    j = lax.axis_index("tp")
    z, x = s // 4, s % 4
    y, c = j // 2, j % 2

    def at(sp, tp):
        return {"sp": sp, "tp": tp}

    def chip_x(by):
        return at(z * 4 + (x + by + 4) % 4, j)

    def chip_z(by):
        return at(((z + by + 4) % 4) * 4 + x, j)

    def chip_y(by):
        return at(s, ((y + by + 4) % 4) * 2 + c)

    def later(by):
        return at((s + by + 16) % 16, j)

    sibling = at(s, y * 2 + 1 - c)

    barrier = pltpu.get_barrier_semaphore()
    partners = [chip_x(1), chip_x(-1), chip_y(1), chip_y(-1), sibling]
    partners += [later(by) for by in (1, 2, 3, 4, -1, -2, -3, -4)]
    for partner in partners:
        pl.semaphore_signal(barrier, inc=1, device_id=partner, device_id_type=MESH)
    pl.semaphore_wait(barrier, len(partners))

    def remote(src, dst, send, recv, device):
        return pltpu.make_async_remote_copy(
            src_ref=src, dst_ref=dst, send_sem=send, recv_sem=recv, device_id=device, device_id_type=MESH
        )

    waiting = []

    def launch(copy):
        copy.start()
        waiting.append(copy)

    gathered = {"up": (w_up, up, send_up, recv_up), "down": (w_down, down, send_down, recv_down)}

    def origin(piece):
        tensor, colour, half, first, second = piece
        dx, dz = (first, second) if colour == 0 else (second, first)
        row = (((z - dz + 4) % 4) * 4 + (x - dx + 4) % 4) * ROWS + colour * 96 + half * UNIT
        return pl.ds(pl.multiple_of(row, UNIT), UNIT)

    def slot(piece):
        tensor, colour, half, first, second = piece
        return ((colour * 2 + half) * 4 + first) * 4 + second

    def begin(start):
        piece, axis, direction = start
        tensor, colour, half, first, second = piece
        source, buffer, send, recv = gathered[tensor]
        if (axis == "x") == (colour == 0):
            landed = (tensor, colour, half, (first + direction) % 4, second)
        else:
            landed = (tensor, colour, half, first, (second + direction) % 4)
        place = origin(piece)
        if first == 0 and second == 0:
            src = source.at[pl.ds(colour * 96 + half * UNIT, UNIT), :]
        else:
            src = buffer.at[place, :]
        device = chip_x(direction) if axis == "x" else chip_z(direction)
        launch(remote(src, buffer.at[place, :], send.at[slot(landed)], recv.at[slot(landed)], device))

    first_starts, events = gather_plan()
    position = [0]

    def pump(stop):
        while position[0] < len(events) and stop(events[position[0]]):
            _, piece, starts = events[position[0]]
            position[0] += 1
            if piece is not None:
                _, buffer, send, recv = gathered[piece[0]]
                place = buffer.at[origin(piece), :]
                remote(place, place, send.at[slot(piece)], recv.at[slot(piece)], sibling).wait_recv()
            for start in starts:
                begin(start)

    def pump_until(time):
        pump(lambda event: event[0] <= time)

    def pump_all(wanted):
        last = max(k for k, event in enumerate(events) if event[1] is not None and wanted(event[1]))
        while position[0] <= last:
            pump(lambda event: event is events[position[0]] and position[0] <= last)

    for start in first_starts:
        begin(start)
    locals_ = [
        pltpu.make_async_copy(w_up, up.at[pl.ds(pl.multiple_of(s * ROWS, ROWS), ROWS), :], local_sem.at[0]),
        pltpu.make_async_copy(w_down, down.at[pl.ds(pl.multiple_of(s * ROWS, ROWS), ROWS), :], local_sem.at[1]),
    ]
    for copy in locals_:
        copy.start()

    lane = lax.broadcasted_iota(jnp.int32, (1, HEADS), 1)
    low = lane < DH
    masks = [jnp.where(low, 1.0, 0.0).astype(BF), jnp.where(low, 0.0, 1.0).astype(BF)]

    seg_row = rows[2:3, :]
    last_seg = rows[2:3, TOKENS - 1 : TOKENS]
    second_seg = rows[2:3, TOKENS - 2 : TOKENS - 1]
    weights = []
    tops = []
    for h in range(2):
        top = jnp.max(jnp.where(seg_row == last_seg, rows[h : h + 1, :], ABSENT), axis=1, keepdims=True)
        inside = cols[:, 2:3] == last_seg
        weights.append(jnp.where(inside, jnp.exp(jnp.where(inside, cols[:, h : h + 1], ABSENT) - top), 0.0))
        tops.append(top)
    total = [rows[3 + h : 4 + h, TOKENS - 1 : TOKENS] for h in range(2)]
    weighted = (keys[...].astype(F32) * jnp.where(low, weights[0], weights[1])).astype(BF)
    product = lax.dot_general(weighted, values[...], TN, preferred_element_type=F32)
    state_out[...] = (jnp.where(low, product[:DH], product[DH:]) * DH**-0.5).astype(BF)
    peak_row = jnp.where(low, tops[0] + total[0], tops[1] + total[1])
    total_row = jnp.where(low, total[0], total[1])
    meta_out[...] = jnp.concatenate(
        [
            peak_row,
            total_row,
            jnp.broadcast_to(last_seg, (1, HEADS)),
            jnp.broadcast_to(second_seg, (1, HEADS)),
            jnp.zeros((4, HEADS), F32),
        ],
        axis=0,
    )
    for by in range(1, 5):
        launch(remote(meta_out, metas.at[by - 1], meta_send.at[by - 1], meta_recv.at[by - 1], later(by)))
        launch(remote(state_out, states.at[by - 1], state_send.at[by - 1], state_recv.at[by - 1], later(by)))

    def local_part(i):
        span = (i + 1) * CHUNK
        here = slice(i * CHUNK, span)
        q = query[here, :]
        ks, vs = keys[:span, :], values[:span, :]
        seg = cols[here, 2:3]
        placed = lax.broadcasted_iota(jnp.int32, (CHUNK, span), 0) + i * CHUNK
        allowed = (placed >= lax.broadcasted_iota(jnp.int32, (CHUNK, span), 1)) & (seg == rows[2:3, :span])
        outs, peaks = [], []
        for h in range(2):
            scores = lax.dot_general(q * masks[h], ks, NT, preferred_element_type=F32)
            log = jnp.where(allowed, rows[h : h + 1, :span], ABSENT)
            peak = jnp.max(log, axis=1, keepdims=True)
            scores = scores * (jnp.exp(log - peak) * DH**-0.5)
            outs.append(jnp.dot(scores.astype(BF), vs, preferred_element_type=F32))
            peaks.append(peak)
        return jnp.where(low, outs[0], outs[1]), jnp.where(low, peaks[0], peaks[1])

    carried = {}

    def receive_state():
        for by in range(1, 5):
            remote(meta_out, metas.at[by - 1], meta_send.at[by - 1], meta_recv.at[by - 1], sibling).wait_recv()
            remote(state_out, states.at[by - 1], state_send.at[by - 1], state_recv.at[by - 1], sibling).wait_recv()
        last_prev = jnp.where(s >= 1, metas[0, 2:3, :], -1.0)
        passed = jnp.zeros((1, HEADS), F32)
        logs = []
        for by in range(1, 5):
            use = (metas[by - 1, 2:3, :] == last_prev) & (s >= by)
            logs.append(jnp.where(use, metas[by - 1, 0:1, :] + passed, ABSENT))
            passed = passed + metas[by - 1, 1:2, :]
        peak = jnp.maximum(jnp.maximum(logs[0], logs[1]), jnp.maximum(logs[2], logs[3]))
        state = jnp.zeros((DH, HEADS), F32)
        for by in range(1, 5):
            coef = jnp.where(logs[by - 1] > 0.5 * ABSENT, jnp.exp(logs[by - 1] - peak), 0.0)
            state = state + coef * states[by - 1].astype(F32)
        carried["state"] = jnp.concatenate(
            [jnp.where(low, state, 0.0), jnp.where(low, 0.0, state)], axis=0
        ).astype(BF)
        carried["peak"] = peak
        carried["last"] = last_prev
        carried["second"] = jnp.where(s >= 1, metas[0, 3:4, :], -1.0)

    def attention(i, local):
        here = slice(i * CHUNK, (i + 1) * CHUNK)
        o, top = local
        inter = jnp.where(cols[here, 2:3] == carried["last"], carried["peak"], ABSENT)
        peak = jnp.maximum(top, inter)
        far = jnp.dot(query[here, :], carried["state"], preferred_element_type=F32)
        o = jnp.exp(top - peak) * o + jnp.exp(inter - peak) * far
        squares = o * o
        sums = [
            jnp.sum(jnp.where(low, squares, 0.0), axis=1, keepdims=True),
            jnp.sum(jnp.where(low, 0.0, squares), axis=1, keepdims=True),
        ]
        norm = jnp.where(low, *[lax.rsqrt(total_ * (1.0 / DH) + HEAD_FLOOR) for total_ in sums])
        mix = (o * norm * head_gain[...] * jax.nn.sigmoid(out_gate[here, :].astype(F32))).astype(BF)
        for k in range(8):
            share[k % 2, k // 2, here, :] = jnp.dot(
                mix, w_out[:, k * OWN : (k + 1) * OWN], preferred_element_type=F32
            ).astype(BF)
        launch(remote(share.at[1 - c, :, here, :], sib.at[:, here, :], sib_send.at[i], sib_recv.at[i], sibling))

    up_y, down_y = chip_y(1), chip_y(-1)
    next_y, prev_y, far_y = (y + 1) % 4, (y + 3) % 4, (y + 2) % 4
    half = CHUNK // 2

    def scatter_first(i):
        here = slice(i * CHUNK, (i + 1) * CHUNK)
        h0 = slice(i * CHUNK, i * CHUNK + half)
        h1 = slice(i * CHUNK + half, (i + 1) * CHUNK)
        n = slice(i * half, (i + 1) * half)
        remote(
            share.at[1 - c, :, here, :], sib.at[:, here, :], sib_send.at[i], sib_recv.at[i], sibling
        ).wait_recv()
        for k in range(4):
            comb[k, here, :] = (
                share[c, k, here, :].astype(F32) + sib[k, here, :].astype(F32)
            ).astype(BF)
        launch(remote(comb.at[far_y, h0, :], near_l.at[n, :], rs_send.at[i, 0], rs_recv.at[i, 0], up_y))
        launch(remote(comb.at[far_y, h1, :], near_r.at[n, :], rs_send.at[i, 1], rs_recv.at[i, 1], down_y))
        launch(remote(comb.at[next_y, h1, :], far_l.at[h1, :], rs_send.at[i, 2], rs_recv.at[i, 2], up_y))
        launch(remote(comb.at[prev_y, h0, :], far_r.at[h0, :], rs_send.at[i, 3], rs_recv.at[i, 3], down_y))

    def scatter_second(i):
        h0 = slice(i * CHUNK, i * CHUNK + half)
        h1 = slice(i * CHUNK + half, (i + 1) * CHUNK)
        n = slice(i * half, (i + 1) * half)
        for place, rows_, buffer, far, k, device in (
            (next_y, h0, near_l, far_l, 0, up_y),
            (prev_y, h1, near_r, far_r, 1, down_y),
        ):
            remote(comb.at[far_y, rows_, :], buffer.at[n, :], rs_send.at[i, k], rs_recv.at[i, k], device).wait_recv()
            comb[place, rows_, :] = (
                comb[place, rows_, :].astype(F32) + buffer[n, :].astype(F32)
            ).astype(BF)
            launch(
                remote(
                    comb.at[place, rows_, :], far.at[rows_, :], rs_send.at[i, 4 + k], rs_recv.at[i, 4 + k], device
                )
            )

    def block(tp):
        return pl.ds(pl.multiple_of(tp * OWN, OWN), OWN)

    mine = block(j)

    def scatter_third(i):
        here = slice(i * CHUNK, (i + 1) * CHUNK)
        h0 = slice(i * CHUNK, i * CHUNK + half)
        h1 = slice(i * CHUNK + half, (i + 1) * CHUNK)
        for rows_, buffer, k in ((h1, far_l, 2), (h0, far_r, 3), (h0, far_l, 4), (h1, far_r, 5)):
            remote(
                comb.at[next_y, rows_, :], buffer.at[rows_, :], rs_send.at[i, k], rs_recv.at[i, k], up_y
            ).wait_recv()
        r = (
            resid[here, :].astype(F32)
            + comb[y, here, :].astype(F32)
            + (far_l[here, :].astype(F32) + far_r[here, :].astype(F32))
        )
        residual[here, :] = r
        normed[here, mine] = (r * own_gain[...]).astype(BF)
        place = normed.at[here, mine]
        launch(remote(place, place, ag_send.at[i, 0], ag_recv.at[i, 0], up_y))
        launch(remote(place, place, ag_send.at[i, 1], ag_recv.at[i, 1], down_y))
        launch(remote(place, place, pass_send.at[i, 0], pass_recv.at[i, 0], sibling))

    def gather_second(i):
        here = slice(i * CHUNK, (i + 1) * CHUNK)
        h0 = slice(i * CHUNK, i * CHUNK + half)
        h1 = slice(i * CHUNK + half, (i + 1) * CHUNK)
        for k, by, rows_, device in ((0, 3, h0, up_y), (1, 1, h1, down_y)):
            column = block(((y + by) % 4) * 2 + c)
            place = normed.at[here, column]
            remote(place, place, ag_send.at[i, k], ag_recv.at[i, k], device).wait_recv()
            part = normed.at[rows_, column]
            launch(remote(part, part, ag_send.at[i, 2 + k], ag_recv.at[i, 2 + k], device))
            launch(remote(place, place, pass_send.at[i, 1 + k], pass_recv.at[i, 1 + k], sibling))

    def gather_third(i):
        h0 = slice(i * CHUNK, i * CHUNK + half)
        h1 = slice(i * CHUNK + half, (i + 1) * CHUNK)
        column = block(far_y * 2 + c)
        for k, rows_ in ((0, h0), (1, h1)):
            part = normed.at[rows_, column]
            remote(part, part, ag_send.at[i, 2 + k], ag_recv.at[i, 2 + k], sibling).wait_recv()
            launch(remote(part, part, pass_send.at[i, 3 + k], pass_recv.at[i, 3 + k], sibling))

    def gather_last(i):
        here = slice(i * CHUNK, (i + 1) * CHUNK)
        h0 = slice(i * CHUNK, i * CHUNK + half)
        h1 = slice(i * CHUNK + half, (i + 1) * CHUNK)
        for k, by, rows_ in ((0, 0, here), (1, 3, here), (2, 1, here), (3, 2, h0), (4, 2, h1)):
            part = normed.at[rows_, block(((y + by) % 4) * 2 + 1 - c)]
            remote(part, part, pass_send.at[i, k], pass_recv.at[i, k], sibling).wait_recv()
        total_ = jnp.zeros((CHUNK, 128), F32)
        for k in range(WIDTH // 128):
            columns = slice(k * 128, (k + 1) * 128)
            part = normed[here, columns].astype(F32) * (1.0 / full_gain[:, columns])
            total_ = total_ + part * part
        mean = jnp.sum(total_, axis=1, keepdims=True) * (1.0 / WIDTH)
        scale[here, :] = jnp.broadcast_to(lax.rsqrt(mean + EPSILON), (CHUNK, 128))

    local0 = local_part(0)
    receive_state()
    attention(0, local0)
    local1 = local_part(1)
    scatter_first(0)
    pump_until(9.0)
    attention(1, local1)
    scatter_second(0)
    local2 = local_part(2)
    scatter_first(1)
    pump_until(16.0)
    attention(2, local2)
    scatter_third(0)
    scatter_second(1)
    scatter_first(2)
    pump_until(22.0)
    gather_second(0)
    scatter_third(1)
    scatter_second(2)
    pump_until(28.0)
    gather_third(0)
    gather_second(1)
    pump_until(33.0)
    scatter_third(2)
    gather_last(0)
    gather_third(1)
    pump_until(40.0)
    gather_second(2)
    gather_last(1)
    pump_until(46.0)
    gather_third(2)
    pump_until(52.0)
    gather_last(2)
    for copy in locals_:
        copy.wait()
    pump_all(lambda piece: piece[0] == "up")

    x_rows = normed

    def product_of(columns, width):
        wide = scale[...] if width == 128 else jnp.concatenate([scale[...]] * (width // 128), axis=1)
        return (jnp.dot(x_rows[...], up[:, columns], preferred_element_type=F32) * wide).astype(BF)

    tail = product_of(slice(2 * MAIN, 2 * MAIN + 128), 128).astype(F32)
    gate_tail[...] = pltpu.roll(tail, 64, 1)
    value_tail[...] = pltpu.roll(tail, 32, 1)

    def up_loop(target, offset):
        @pl.loop(0, 4)
        def _(n):
            columns = pl.ds(pl.multiple_of(n * 256, 256), 256)
            source = pl.ds(pl.multiple_of(n * 256 + offset, 256), 256)
            target[:, columns] = product_of(source, 256)

    now = max(event[0] for event in events if event[1] is not None and event[1][0] == "up")
    up_loop(gate, 0)
    edge_out[...] = gate[TOKENS - 16 :, :]
    edge_tail_out[...] = gate_tail[TOKENS - 16 :, :]
    launch(remote(edge_out, edge, edge_send.at[0], edge_recv.at[0], later(1)))
    launch(remote(edge_tail_out, edge_tail, edge_send.at[1], edge_recv.at[1], later(1)))
    pump_until(now + 7.0)
    up_loop(value, MAIN)
    pump_until(now + 14.0)
    remote(edge_out, edge, edge_send.at[0], edge_recv.at[0], sibling).wait_recv()
    remote(edge_tail_out, edge_tail, edge_send.at[1], edge_recv.at[1], sibling).wait_recv()

    seg = cols[:, 2:3]
    place = lax.broadcasted_iota(jnp.int32, (TOKENS, 1), 0)
    last_one, second_one = carried["last"][:, 0:1], carried["second"][:, 0:1]
    before = jnp.where(place == 0, last_one, cols[:, 3:4])
    before_two = jnp.where(place == 0, second_one, jnp.where(place == 1, last_one, cols[:, 4:5]))
    near_mask = jnp.where(before == seg, 1.0, 0.0)
    far_mask = jnp.where(before_two == seg, 1.0, 0.0)
    wide_near = jnp.broadcast_to(near_mask, (TOKENS, 128)) > 0.5
    wide_far = jnp.broadcast_to(far_mask, (TOKENS, 128)) > 0.5
    at_first = jnp.broadcast_to(place, (TOKENS, 128)) == 0
    at_second = jnp.broadcast_to(place, (TOKENS, 128)) == 1

    def mixed(g, v, tap, previous):
        one = jnp.where(at_first, previous[15:16, :], pltpu.roll(g, 1, 0))
        two = jnp.where(
            at_first, previous[14:15, :], jnp.where(at_second, previous[15:16, :], pltpu.roll(g, 2, 0))
        )
        conv = (
            tap[2:3, :] * g
            + tap[1:2, :] * jnp.where(wide_near, one, 0.0)
            + tap[0:1, :] * jnp.where(wide_far, two, 0.0)
        )
        return (conv * jax.nn.sigmoid(conv) * v).astype(BF)

    lanes = lax.broadcasted_iota(jnp.int32, (TOKENS, 128), 1)
    inside = (lanes >= 64) & (lanes < 96)
    hidden_tail[...] = jnp.where(
        inside, mixed(gate_tail[...], value_tail[...], tap_tail[...], edge_tail[...]).astype(F32), 0.0
    ).astype(BF)

    @pl.loop(0, MAIN // 128)
    def _(n):
        columns = pl.ds(pl.multiple_of(n * 128, 128), 128)
        hidden[:, columns] = mixed(
            gate[:, columns].astype(F32),
            value[:, columns].astype(F32),
            taps[:, columns],
            edge[:, columns].astype(F32),
        )

    pump_until(now + 20.0)

    dhalf = TOKENS // 2
    d0, d1 = slice(0, dhalf), slice(dhalf, TOKENS)

    def origin_z(piece):
        return piece[4] if piece[1] == 0 else piece[3]

    def down_product(g, dz):
        pump_all(lambda piece: piece[0] == "down" and origin_z(piece) == dz)
        target = (z - dz + 4) % 4
        for side in range(2):
            place = pl.ds(pl.multiple_of(target * 2 * OWN + side * OWN, OWN), OWN)
            dshare[g, side, :, :] = (
                lax.dot_general(hidden[...], down[place, :], NT, preferred_element_type=F32)
                + lax.dot_general(
                    hidden_tail[...], up[place, 2 * MAIN :], NT, preferred_element_type=F32
                )
            ).astype(BF)
        launch(remote(dshare.at[g, 1 - c], dsib.at[g], dsib_send.at[g], dsib_recv.at[g], sibling))
        return target

    near_l_copy = lambda src: remote(src, dnear_l, drs_send.at[0], drs_recv.at[0], up_y)
    near_r_copy = lambda src: remote(src, dnear_r, drs_send.at[1], drs_recv.at[1], down_y)
    far_copies = {
        "l1": lambda src: remote(src, dfar_l.at[d1, :], drs_send.at[2], drs_recv.at[2], up_y),
        "r0": lambda src: remote(src, dfar_r.at[d0, :], drs_send.at[3], drs_recv.at[3], down_y),
        "l0": lambda src: remote(src, dfar_l.at[d0, :], drs_send.at[4], drs_recv.at[4], up_y),
        "r1": lambda src: remote(src, dfar_r.at[d1, :], drs_send.at[5], drs_recv.at[5], down_y),
    }

    def down_combine(g, target):
        remote(dshare.at[g, 1 - c], dsib.at[g], dsib_send.at[g], dsib_recv.at[g], sibling).wait_recv()
        dcomb[target] = (dshare[g, c].astype(F32) + dsib[g].astype(F32)).astype(BF)

        @pl.when(target == far_y)
        def _():
            near_l_copy(dcomb.at[far_y, d0, :]).start()
            near_r_copy(dcomb.at[far_y, d1, :]).start()

        @pl.when(target == next_y)
        def _():
            far_copies["l1"](dcomb.at[next_y, d1, :]).start()

        @pl.when(target == prev_y)
        def _():
            far_copies["r0"](dcomb.at[prev_y, d0, :]).start()

    def down_relay(target):
        @pl.when(target == next_y)
        def _():
            near_l_copy(dcomb.at[far_y, d0, :]).wait_recv()
            dcomb[next_y, d0, :] = (dcomb[next_y, d0, :].astype(F32) + dnear_l[...].astype(F32)).astype(BF)
            far_copies["l0"](dcomb.at[next_y, d0, :]).start()

        @pl.when(target == prev_y)
        def _():
            near_r_copy(dcomb.at[far_y, d1, :]).wait_recv()
            dcomb[prev_y, d1, :] = (dcomb[prev_y, d1, :].astype(F32) + dnear_r[...].astype(F32)).astype(BF)
            far_copies["r1"](dcomb.at[prev_y, d1, :]).start()

    targets = []
    for g, dz in enumerate((0, 1, 3, 2)):
        targets.append(down_product(g, dz))
        if g >= 1:
            down_combine(g - 1, targets[g - 1])
        if g >= 2:
            down_relay(targets[g - 2])
    down_combine(3, targets[3])
    down_relay(targets[2])
    down_relay(targets[3])
    for name, buffer, rows_ in (("l1", dfar_l, d1), ("r0", dfar_r, d0), ("l0", dfar_l, d0), ("r1", dfar_r, d1)):
        far_copies[name](buffer.at[rows_, :]).wait_recv()
    out[...] = (
        residual[...]
        + dcomb[y].astype(F32)
        + (dfar_l[...].astype(F32) + dfar_r[...].astype(F32))
    ).astype(BF)

    near_l_copy(dcomb.at[far_y, d0, :]).wait_send()
    near_r_copy(dcomb.at[far_y, d1, :]).wait_send()
    for name, where_, rows_ in (("l1", next_y, d1), ("r0", prev_y, d0), ("l0", next_y, d0), ("r1", prev_y, d1)):
        far_copies[name](dcomb.at[where_, rows_, :]).wait_send()
    for copy in waiting:
        copy.wait_send()


def body(
    resid, query, keys, values, out_gate, in_gate, forget, doc_ids, head_gain, w_out, ffn_gain,
    w_gate, w_value, conv_taps, w_down,
):
    seg = doc_ids.astype(F32)
    cumul = jnp.cumsum(jax.nn.log_sigmoid(forget), axis=1)
    gain_in = in_gate - cumul
    rows = jnp.concatenate([gain_in, seg[None], cumul, jnp.zeros((3, TOKENS), F32)], axis=0)
    absent = jnp.full((2,), -1.0, F32)
    back = jnp.concatenate([absent, seg])
    cols = jnp.stack(
        [gain_in[0], gain_in[1], seg, back[1:-1], back[:-2], seg, seg, seg], axis=1
    )
    turned = w_down.T
    tails = jnp.concatenate(
        [w_gate[:, MAIN:], w_value[:, MAIN:], turned[:, MAIN:], jnp.zeros((ROWS, 32), BF)], axis=1
    )
    w_up = jnp.concatenate([w_gate[:, :MAIN], w_value[:, :MAIN], tails], axis=1)
    w_low = turned[:, :MAIN]
    taps = conv_taps[:, :MAIN]
    tap_tail = jnp.pad(conv_taps[:, MAIN:], ((0, 0), (64, 32)))
    own_gain = lax.dynamic_slice_in_dim(ffn_gain, lax.axis_index("tp") * OWN, OWN, 0)

    vmem = pl.BlockSpec(memory_space=pltpu.VMEM)
    hbm = pl.BlockSpec(memory_space=pl.ANY)
    dma = pltpu.SemaphoreType.DMA
    scratch = [
        pltpu.VMEM((WIDTH, 2 * MAIN + 128), BF),
        pltpu.VMEM((WIDTH, MAIN), BF),
        pltpu.VMEM((TOKENS, WIDTH), BF),
        pltpu.VMEM((2, 4, TOKENS, OWN), BF),
        pltpu.VMEM((4, TOKENS, OWN), BF),
        pltpu.VMEM((4, TOKENS, OWN), BF),
        pltpu.VMEM((TOKENS // 2, OWN), BF),
        pltpu.VMEM((TOKENS // 2, OWN), BF),
        pltpu.VMEM((TOKENS, OWN), BF),
        pltpu.VMEM((TOKENS, OWN), BF),
        pltpu.VMEM((TOKENS, OWN), F32),
        pltpu.VMEM((TOKENS, MAIN), BF),
        pltpu.VMEM((TOKENS, MAIN), BF),
        pltpu.VMEM((TOKENS, 128), F32),
        pltpu.VMEM((TOKENS, 128), F32),
        pltpu.VMEM((TOKENS, MAIN), BF),
        pltpu.VMEM((TOKENS, 128), BF),
        pltpu.VMEM((16, MAIN), BF),
        pltpu.VMEM((16, 128), F32),
        pltpu.VMEM((16, MAIN), BF),
        pltpu.VMEM((16, 128), F32),
        pltpu.VMEM((TOKENS, 128), F32),
        pltpu.VMEM((DH, HEADS), BF),
        pltpu.VMEM((8, HEADS), F32),
        pltpu.VMEM((4, DH, HEADS), BF),
        pltpu.VMEM((4, 8, HEADS), F32),
        pltpu.VMEM((4, 2, TOKENS, OWN), BF),
        pltpu.VMEM((4, TOKENS, OWN), BF),
        pltpu.VMEM((4, TOKENS, OWN), BF),
        pltpu.VMEM((TOKENS // 2, OWN), BF),
        pltpu.VMEM((TOKENS // 2, OWN), BF),
        pltpu.VMEM((TOKENS, OWN), BF),
        pltpu.VMEM((TOKENS, OWN), BF),
        dma((64,)),
        dma((64,)),
        dma((64,)),
        dma((64,)),
        dma((2,)),
        dma((4,)),
        dma((4,)),
        dma((4,)),
        dma((4,)),
        dma((2,)),
        dma((2,)),
        dma((CHUNKS,)),
        dma((CHUNKS,)),
        dma((CHUNKS, 6)),
        dma((CHUNKS, 6)),
        dma((CHUNKS, 4)),
        dma((CHUNKS, 4)),
        dma((CHUNKS, 5)),
        dma((CHUNKS, 5)),
        dma((4,)),
        dma((4,)),
        dma((6,)),
        dma((6,)),
    ]
    return pl.pallas_call(
        layer_kernel,
        in_specs=[vmem] * 11 + [hbm] * 2 + [vmem] * 2,
        out_specs=vmem,
        out_shape=jax.ShapeDtypeStruct((TOKENS, OWN), BF),
        scratch_shapes=scratch,
        compiler_params=pltpu.CompilerParams(
            collective_id=0, has_side_effects=True, vmem_limit_bytes=67043328
        ),
        name="layer",
    )(
        resid, query, keys, values, out_gate, cols, rows, head_gain[None], w_out, own_gain[None],
        ffn_gain[None], w_up, w_low, taps, tap_tail,
    )


def solution(mesh):
    placed = (
        P("sp", "tp"),
        P("sp", "tp"),
        P("sp", "tp"),
        P("sp", "tp"),
        P("sp", "tp"),
        P("tp", "sp"),
        P("tp", "sp"),
        P("sp"),
        P("tp"),
        P("tp", None),
        P(),
        P("sp", "tp"),
        P("sp", "tp"),
        P(None, "tp"),
        P("tp", "sp"),
    )
    return jax.shard_map(body, mesh=mesh, in_specs=placed, out_specs=P("sp", "tp"), check_vma=False)
```

profile of v0, /device:TPU:16, one launch (start us, length us, event | category | flops | bytes accessed | tf_op | source)
XLA Modules:
  0.0 191.5 jit_solution(13792508601253324922)
XLA Ops:
  0.0 0.7 fusion
  0.7 0.6 reduce-window.6
  1.3 0.2 slice_reduce_fusion
  1.5 0.2 reduce-window.9
  1.7 0.1 add_bitcast_fusion
  1.7 0.7 fusion.1
  2.4 0.7 convert_element_type.5
  3.1 0.1 pad_slice_fusion
  3.2 0.1 stack.18
  3.3 0.0 slice-start
  3.3 0.0 slice-start.1
  3.3 0.0 slice-start.2
  3.3 0.0 slice-start.3
  3.3 0.9 copy.36.cols
  4.3 0.1 pad.9.clone
  4.4 0.7 maximum_maximum_fusion.rows
  5.0 0.8 dynamic_slice.3
  5.8 0.6 broadcast_in_dim.21.own_gain
  6.4 0.8 slice.59
  7.2 0.0 copy-start.1
  7.3 1.1 concatenate.11.w_up
  8.4 0.8 slice.60.w_down
  9.2 0.9 copy.32.query
  10.1 0.9 copy.33.keys
  11.0 0.0 copy-done.3
  11.0 1.0 copy.34.values
  12.0 0.9 copy.35.out_gate
  12.9 0.6 slice.54.taps
  13.5 0.0 slice-done.4
  13.5 0.6 pad.5.tap_tail
  14.2 175.4 %layer.1 = bf16[768,384]{1,0:T(8,128)(2,1)} custom-call(bf16[768,384]{1,0:T(8,128)(2,1)} %resid.1, bf16[768,192]{1,0:T(8,128)(2,1)} %copy.32.query, bf16[768,192]{1,0:T(8,128)(2,1)} %copy.33.keys, bf16[768,192]{1,0:T(8,128)(2,1)} %copy.34.values, bf16[768,192]{1,0:T(8,128)(2,1)} %copy.35.out_gate, f32[768,8]{1,0:T(8,128)} %copy.36.cols, ...), custom_call_target="tpu_custom_call" | custom-call | tf_op jit(solution)/shard_map/layer/pallas_call | solution.py:688
  189.6 1.9 %copy.41 = bf16[768,384]{1,0:T(8,128)(2,1)} copy(bf16[768,384]{1,0:T(8,128)(2,1)} %layer.1) | data formatting | bytes 1179648
  (23 shorter events, 0.1 us)
Async XLA Ops:
  3.3 3.9 %slice-start = ((bf16[192,1056]{1,0:T(8,128)(2,1)}), bf16[192,1024]{1,0:T(8,128)(2,1)S(1)}, s32[]{:S(2)}) async-start(bf16[192,1056]{1,0:T(8,128)(2,1)} %param.26), calls=%async_computation | async-start | bytes 786432 | tf_op jit(solution)/shard_map/slice | solution.py:621
  3.3 3.9 %slice-start.1 = ((bf16[192,1056]{1,0:T(8,128)(2,1)}), bf16[192,32]{1,0:T(8,128)(2,1)S(1)}, s32[]{:S(2)}) async-start(bf16[192,1056]{1,0:T(8,128)(2,1)} %param.26), calls=%async_computation.1 | async-start | bytes 98304 | tf_op jit(solution)/shard_map/slice | solution.py:619
  3.3 3.9 %slice-start.2 = ((bf16[192,1056]{1,0:T(8,128)(2,1)}), bf16[192,1024]{1,0:T(8,128)(2,1)S(1)}, s32[]{:S(2)}) async-start(bf16[192,1056]{1,0:T(8,128)(2,1)} %param.27), calls=%async_computation.2 | async-start | bytes 786432 | tf_op jit(solution)/shard_map/slice | solution.py:621
  3.3 3.9 %slice-start.3 = ((bf16[192,1056]{1,0:T(8,128)(2,1)}), bf16[192,32]{1,0:T(8,128)(2,1)S(1)}, s32[]{:S(2)}) async-start(bf16[192,1056]{1,0:T(8,128)(2,1)} %param.27), calls=%async_computation.3 | async-start | bytes 98304 | tf_op jit(solution)/shard_map/slice | solution.py:619
  7.2 1.2 copy-start
  7.2 1.9 %copy-start.1 = (bf16[768,192]{0,1:T(8,128)(2,1)S(1)}, bf16[768,192]{0,1:T(8,128)(2,1)}, u32[]{:S(2)}) copy-start(bf16[768,192]{0,1:T(8,128)(2,1)} %param.16) | copy-start | bytes 884740
  8.4 1.7 copy-start.2
  8.4 2.7 %copy-start.3 = (bf16[768,192]{0,1:T(8,128)(2,1)S(1)}, bf16[768,192]{0,1:T(8,128)(2,1)}, u32[]{:S(2)}) copy-start(bf16[768,192]{0,1:T(8,128)(2,1)} %param.18) | copy-start | bytes 884740
  9.2 2.8 %copy-start.4 = (bf16[768,192]{0,1:T(8,128)(2,1)S(1)}, bf16[768,192]{0,1:T(8,128)(2,1)}, u32[]{:S(2)}) copy-start(bf16[768,192]{0,1:T(8,128)(2,1)} %param.19) | copy-start | bytes 884740
  10.1 2.8 %copy-start.5 = (f32[3,1056]{1,0:T(4,128)S(1)}, f32[3,1056]{1,0:T(4,128)}, u32[]{:S(2)}) copy-start(f32[3,1056]{1,0:T(4,128)} %param.28) | copy-start | bytes 38020
  10.1 3.4 %slice-start.4 = ((f32[3,1056]{1,0:T(4,128)}), f32[3,32]{1,0:T(4,128)S(1)}, s32[]{:S(2)}) async-start(f32[3,1056]{1,0:T(4,128)} %param.28), calls=%async_computation.4 | async-start | bytes 4096 | tf_op jit(solution)/shard_map/slice | solution.py:624
where the time goes:
time: 194 us; the launch traced here: 192 us
  Pallas kernels  175 us (90%)
  local copies, waits for them, and re-layouts  12.4 us (6%)
  other arithmetic  3.62 us (2%)
    pallas_call x1, Pallas kernels, body(): pl.pallas_call(layer_kernel, in_specs=[vmem] * 11 + [hbm] * 2 + [vmem] *...  175 us
    unnamed x17, local copies, waits for them, and re-layouts  5.67 us

commit v1 on v0

v1 whole, which is shorter than its diff:
```python
import heapq

import jax
import jax.numpy as jnp
from jax import lax
from jax.experimental import pallas as pl
from jax.experimental.pallas import tpu as pltpu
from jax.sharding import PartitionSpec as P

DH = 96
ABSENT = -1e30
EPSILON = 1e-06
HEAD_FLOOR = 1.0
TOKENS = 768
WIDTH = 3072
ROWS = 192
OWN = 384
HEADS = 192
MAIN = 1024
CHUNK = 256
CHUNKS = TOKENS // CHUNK
UNIT = 48
KINDS = ("near_l", "near_r", "l1", "r0", "l0", "r1")
COMBINE_LAG = 2
RELAY_LAG = 6
BF = jnp.bfloat16
F32 = jnp.float32
MESH = pl.DeviceIdType.MESH
NT = (((1,), (1,)), ((), ()))
TN = (((0,), (0,)), ((), ()))

RATES = {"up": 4.6, "down": 2.2}
HOP = 2.2
LEAD = 9.0
LATE = {3: 0, 1: 1, 2: 2, 0: 3}


def axes(colour):
    return ("x", "z") if colour == 0 else ("z", "x")


def landing(start):
    (tensor, colour, half, first, second), axis, direction = start
    if axis == axes(colour)[0]:
        return (tensor, colour, half, (first + direction) % 4, second)
    return (tensor, colour, half, first, (second + direction) % 4)


def follow(piece):
    tensor, colour, half, first, second = piece
    ahead = 1 if half == 0 else -1
    one, two = axes(colour)
    if first == 0 and second == 0:
        return [(piece, axis, way) for axis in (one, two) for way in (ahead, -ahead)]
    if second == 0:
        starts = [(piece, two, ahead), (piece, two, -ahead)]
        return starts + ([(piece, one, ahead)] if first == ahead % 4 else [])
    return [(piece, two, ahead)] if second == ahead % 4 else []


def depth(start):
    return 1 + max([depth(then) for then in follow(landing(start))] or [0])


def urgency(start):
    tensor, colour, half, first, second = landing(start)
    if tensor == "up":
        return (0, -depth(start), half)
    if second == 0:
        return (1, 0, -depth(start))
    if colour == 0:
        return (1, 1, 0 if start[2] == (1 if half == 0 else -1) else 1, -depth(start))
    return (1, 1, LATE[first], -depth(start))


def gather_plan():
    ready = {(axis, way): [] for axis in "xz" for way in (1, -1)}
    busy = dict.fromkeys(ready, 0.0)
    arrivals, actions, count, now = [], [], 0, 0.0

    def add(time, piece):
        nonlocal count
        for start in follow(piece):
            count += 1
            heapq.heappush(ready[start[1:]], (urgency(start), count, time, start))

    for tensor in ("up", "down"):
        for colour in (0, 1):
            for half in (0, 1):
                add(0.0, (tensor, colour, half, 0, 0))
    while True:
        for link in ready:
            if busy[link] <= now and ready[link]:
                _, _, since, start = heapq.heappop(ready[link])
                busy[link] = now + RATES[start[0][0]]
                count += 1
                heapq.heappush(arrivals, (busy[link] + HOP, count, landing(start)))
                actions.append((max(since, now - LEAD), 1, count, start))
        times = [busy[link] for link in ready if ready[link]] + [entry[0] for entry in arrivals[:1]]
        if not times:
            return sorted(actions, key=lambda action: action[:3])
        now = min(times)
        while arrivals and arrivals[0][0] <= now:
            time, count_, piece = heapq.heappop(arrivals)
            actions.append((time, 0, count_, piece))
            add(time, piece)


def layer_kernel(
    resid_hbm, query_hbm, keys_hbm, values_hbm, out_gate_hbm, in_gate_hbm, forget_hbm, docs_hbm, head_gain_hbm,
    w_out_hbm, full_gain_hbm, w_gate_hbm, w_value_hbm, taps_hbm, w_down_hbm,
    out,
    resid, query, keys, values, out_gate, in_gate, forget, docs, head_gain, w_out, full_gain, taps,
    stage_gate, stage_value, stage_down, columns_of,
    up, down, normed, share, sib, comb, near_l, near_r, far_l, far_r, residual,
    gate, value, gate_tail, value_tail, hidden, hidden_tail, edge, edge_tail, edge_out, edge_tail_out,
    scale, state_out, meta_out, states, metas,
    dshare, dsib, dcomb, dnear_l, dnear_r, dfar_l, dfar_r,
    load_sem, send_up, recv_up, send_down, recv_down,
    state_send, state_recv, meta_send, meta_recv, edge_send, edge_recv,
    sib_send, sib_recv, rs_send, rs_recv, ag_send, ag_recv, pass_send, pass_recv,
    dsib_send, dsib_recv, drs_send, drs_recv,
):
    s = lax.axis_index("sp")
    j = lax.axis_index("tp")
    z, x = s // 4, s % 4
    y, c = j // 2, j % 2

    def at(sp, tp):
        return {"sp": sp, "tp": tp}

    def chip_x(by):
        return at(z * 4 + (x + by + 4) % 4, j)

    def chip_z(by):
        return at(((z + by + 4) % 4) * 4 + x, j)

    def chip_y(by):
        return at(s, ((y + by + 4) % 4) * 2 + c)

    def later(by):
        return at((s + by + 16) % 16, j)

    sibling = at(s, y * 2 + 1 - c)

    barrier = pltpu.get_barrier_semaphore()
    partners = [chip_x(1), chip_x(-1), chip_y(1), chip_y(-1), sibling]
    partners += [later(by) for by in (1, 2, 3, 4, -1, -2, -3, -4)]
    for partner in partners:
        pl.semaphore_signal(barrier, inc=1, device_id=partner, device_id_type=MESH)

    own_rows = pl.ds(pl.multiple_of(s * ROWS, ROWS), ROWS)
    loads = [
        pltpu.make_async_copy(src, dst, load_sem.at[k])
        for k, (src, dst) in enumerate(
            (
                (forget_hbm, forget),
                (in_gate_hbm, in_gate),
                (docs_hbm, docs),
                (keys_hbm, keys),
                (values_hbm, values),
                (query_hbm, query),
                (w_gate_hbm, stage_gate),
                (w_value_hbm, stage_value),
                (w_down_hbm, stage_down),
                (w_gate_hbm.at[:, :MAIN], up.at[own_rows, :MAIN]),
                (w_value_hbm.at[:, :MAIN], up.at[own_rows, MAIN : 2 * MAIN]),
                (w_down_hbm.at[:, :MAIN], down.at[own_rows, :]),
                (out_gate_hbm, out_gate),
                (head_gain_hbm, head_gain),
                (w_out_hbm, w_out),
                (resid_hbm, resid),
                (full_gain_hbm, full_gain),
                (taps_hbm, taps),
            )
        )
    ]
    for copy in loads:
        copy.start()

    def remote(src, dst, send, recv, device):
        return pltpu.make_async_remote_copy(
            src_ref=src, dst_ref=dst, send_sem=send, recv_sem=recv, device_id=device, device_id_type=MESH
        )

    waiting = []

    def launch(copy):
        copy.start()
        waiting.append(copy)

    gathered = {"up": (up, send_up, recv_up), "down": (down, send_down, recv_down)}

    def origin(piece):
        tensor, colour, half, first, second = piece
        dx, dz = (first, second) if colour == 0 else (second, first)
        row = (((z - dz + 4) % 4) * 4 + (x - dx + 4) % 4) * ROWS + colour * 96 + half * UNIT
        return pl.ds(pl.multiple_of(row, UNIT), UNIT)

    def slot(piece):
        tensor, colour, half, first, second = piece
        return ((colour * 2 + half) * 4 + first) * 4 + second

    def begin(start):
        piece, axis, direction = start
        buffer, send, recv = gathered[piece[0]]
        place = buffer.at[origin(piece), :]
        k = slot(landing(start))
        launch(remote(place, place, send.at[k], recv.at[k], (chip_x if axis == "x" else chip_z)(direction)))

    actions = gather_plan()
    position = [0]
    arrived = set()

    def step():
        _, kind, _, item = actions[position[0]]
        position[0] += 1
        if kind == 1:
            begin(item)
        else:
            buffer, send, recv = gathered[item[0]]
            place = buffer.at[origin(item), :]
            remote(place, place, send.at[slot(item)], recv.at[slot(item)], sibling).wait_recv()
            arrived.add(item)

    def pump_until(time):
        while position[0] < len(actions) and actions[position[0]][0] <= time:
            step()

    def pump_all(wanted):
        last = max(k for k, action in enumerate(actions) if action[1] == 0 and wanted(action[3]))
        while position[0] <= last:
            step()

    lane = lax.broadcasted_iota(jnp.int32, (1, HEADS), 1)
    low = lane < DH
    for k in range(5):
        loads[k].wait()

    f = jnp.concatenate([forget[...], jnp.zeros((6, TOKENS), F32)], axis=0)
    cumul = -(jnp.maximum(-f, 0.0) + jnp.log1p(jnp.exp(-jnp.abs(f))))
    token = lax.broadcasted_iota(jnp.int32, (8, TOKENS), 1)
    for k in range(10):
        if 1 << k < TOKENS:
            cumul = cumul + jnp.where(token >= 1 << k, pltpu.roll(cumul, 1 << k, 1), 0.0)
    seg_row = docs[...].astype(F32)
    g_rows = [in_gate[h : h + 1, :] - cumul[h : h + 1, :] for h in range(2)]
    last_seg = seg_row[:, TOKENS - 1 : TOKENS]
    second_seg = seg_row[:, TOKENS - 2 : TOKENS - 1]
    inside = seg_row == last_seg
    products, tops = [], []
    for h in range(2):
        log = jnp.where(inside, g_rows[h], ABSENT)
        top = jnp.max(log, axis=1, keepdims=True)
        weight = jnp.where(inside, jnp.exp(log - top), 0.0)
        weighted = (keys[h * DH : (h + 1) * DH, :].astype(F32) * weight).astype(BF)
        products.append(lax.dot_general(weighted, values[...], NT, preferred_element_type=F32))
        tops.append(top)
    total = [cumul[h : h + 1, TOKENS - 1 : TOKENS] for h in range(2)]
    state_out[...] = (jnp.where(low, *products) * DH**-0.5).astype(BF)
    meta_out[...] = jnp.concatenate(
        [
            jnp.where(low, tops[0] + total[0], tops[1] + total[1]),
            jnp.where(low, total[0], total[1]),
            jnp.broadcast_to(last_seg, (1, HEADS)),
            jnp.broadcast_to(second_seg, (1, HEADS)),
            jnp.zeros((4, HEADS), F32),
        ],
        axis=0,
    )
    flat = jnp.broadcast_to(seg_row, (8, TOKENS))
    columns_of[...] = jnp.transpose(
        jnp.concatenate(
            [
                seg_row,
                pltpu.roll(flat, 1, 1)[0:1, :],
                pltpu.roll(flat, 2, 1)[0:1, :],
                jnp.zeros((125, TOKENS), F32),
            ],
            axis=0,
        )
    )
    for k in range(5, 12):
        loads[k].wait()
    up[own_rows, 2 * MAIN :] = jnp.concatenate(
        [stage_gate[:, MAIN:], stage_value[:, MAIN:], stage_down[:, MAIN:], jnp.zeros((ROWS, 32), BF)], axis=1
    )

    pl.semaphore_wait(barrier, len(partners))
    for by in range(1, 5):
        launch(remote(meta_out, metas.at[by - 1], meta_send.at[by - 1], meta_recv.at[by - 1], later(by)))
        launch(remote(state_out, states.at[by - 1], state_send.at[by - 1], state_recv.at[by - 1], later(by)))
    pump_until(0.0)

    def local_part(i):
        span = (i + 1) * CHUNK
        here = slice(i * CHUNK, span)
        seg = columns_of[here, 0:1]
        placed = lax.broadcasted_iota(jnp.int32, (CHUNK, span), 0) + i * CHUNK
        allowed = (placed >= lax.broadcasted_iota(jnp.int32, (CHUNK, span), 1)) & (seg == seg_row[:, :span])
        outs, peaks = [], []
        for h in range(2):
            part = slice(h * DH, (h + 1) * DH)
            scores = lax.dot_general(query[part, here], keys[part, :span], TN, preferred_element_type=F32)
            log = jnp.where(allowed, g_rows[h][:, :span], ABSENT)
            peak = jnp.max(log, axis=1, keepdims=True)
            scores = scores * (jnp.exp(log - peak) * DH**-0.5)
            outs.append(lax.dot_general(scores.astype(BF), values[:, :span], NT, preferred_element_type=F32))
            peaks.append(peak)
        return jnp.where(low, outs[0], outs[1]), jnp.where(low, peaks[0], peaks[1])

    carried = {}

    def receive_state():
        for by in range(1, 5):
            remote(meta_out, metas.at[by - 1], meta_send.at[by - 1], meta_recv.at[by - 1], sibling).wait_recv()
            remote(state_out, states.at[by - 1], state_send.at[by - 1], state_recv.at[by - 1], sibling).wait_recv()
        last_prev = jnp.where(s >= 1, metas[0, 2:3, :], -1.0)
        passed = jnp.zeros((1, HEADS), F32)
        logs = []
        for by in range(1, 5):
            use = (metas[by - 1, 2:3, :] == last_prev) & (s >= by)
            logs.append(jnp.where(use, metas[by - 1, 0:1, :] + passed, ABSENT))
            passed = passed + metas[by - 1, 1:2, :]
        peak = jnp.maximum(jnp.maximum(logs[0], logs[1]), jnp.maximum(logs[2], logs[3]))
        state = jnp.zeros((DH, HEADS), F32)
        for by in range(1, 5):
            coef = jnp.where(logs[by - 1] > 0.5 * ABSENT, jnp.exp(logs[by - 1] - peak), 0.0)
            state = state + coef * states[by - 1].astype(F32)
        carried["state"] = jnp.concatenate(
            [jnp.where(low, state, 0.0), jnp.where(low, 0.0, state)], axis=0
        ).astype(BF)
        carried["peak"] = peak
        carried["last"] = last_prev
        carried["second"] = jnp.where(s >= 1, metas[0, 3:4, :], -1.0)

    def attention(i, local):
        here = slice(i * CHUNK, (i + 1) * CHUNK)
        o, top = local
        inter = jnp.where(columns_of[here, 0:1] == carried["last"], carried["peak"], ABSENT)
        peak = jnp.maximum(top, inter)
        far = lax.dot_general(query[:, here], carried["state"], TN, preferred_element_type=F32)
        o = jnp.exp(top - peak) * o + jnp.exp(inter - peak) * far
        squares = o * o
        sums = [
            jnp.sum(jnp.where(low, squares, 0.0), axis=1, keepdims=True),
            jnp.sum(jnp.where(low, 0.0, squares), axis=1, keepdims=True),
        ]
        norm = jnp.where(low, *[lax.rsqrt(total_ * (1.0 / DH) + HEAD_FLOOR) for total_ in sums])
        opened = jnp.transpose(jax.nn.sigmoid(out_gate[:, here].astype(F32)))
        mix = (o * norm * head_gain[...] * opened).astype(BF)
        for k in range(8):
            share[k % 2, k // 2, here, :] = jnp.dot(
                mix, w_out[:, k * OWN : (k + 1) * OWN], preferred_element_type=F32
            ).astype(BF)
        launch(remote(share.at[1 - c, :, here, :], sib.at[:, here, :], sib_send.at[i], sib_recv.at[i], sibling))

    up_y, down_y = chip_y(1), chip_y(-1)
    next_y, prev_y, far_y = (y + 1) % 4, (y + 3) % 4, (y + 2) % 4
    half = CHUNK // 2

    def scatter_first(i):
        here = slice(i * CHUNK, (i + 1) * CHUNK)
        h0 = slice(i * CHUNK, i * CHUNK + half)
        h1 = slice(i * CHUNK + half, (i + 1) * CHUNK)
        n = slice(i * half, (i + 1) * half)
        remote(
            share.at[1 - c, :, here, :], sib.at[:, here, :], sib_send.at[i], sib_recv.at[i], sibling
        ).wait_recv()
        for k in range(4):
            comb[k, here, :] = (
                share[c, k, here, :].astype(F32) + sib[k, here, :].astype(F32)
            ).astype(BF)
        launch(remote(comb.at[far_y, h0, :], near_l.at[n, :], rs_send.at[i, 0], rs_recv.at[i, 0], up_y))
        launch(remote(comb.at[far_y, h1, :], near_r.at[n, :], rs_send.at[i, 1], rs_recv.at[i, 1], down_y))
        launch(remote(comb.at[next_y, h1, :], far_l.at[h1, :], rs_send.at[i, 2], rs_recv.at[i, 2], up_y))
        launch(remote(comb.at[prev_y, h0, :], far_r.at[h0, :], rs_send.at[i, 3], rs_recv.at[i, 3], down_y))

    def scatter_second(i):
        h0 = slice(i * CHUNK, i * CHUNK + half)
        h1 = slice(i * CHUNK + half, (i + 1) * CHUNK)
        n = slice(i * half, (i + 1) * half)
        for place, rows_, buffer, far, k, device in (
            (next_y, h0, near_l, far_l, 0, up_y),
            (prev_y, h1, near_r, far_r, 1, down_y),
        ):
            remote(comb.at[far_y, rows_, :], buffer.at[n, :], rs_send.at[i, k], rs_recv.at[i, k], device).wait_recv()
            comb[place, rows_, :] = (
                comb[place, rows_, :].astype(F32) + buffer[n, :].astype(F32)
            ).astype(BF)
            launch(
                remote(
                    comb.at[place, rows_, :], far.at[rows_, :], rs_send.at[i, 4 + k], rs_recv.at[i, 4 + k], device
                )
            )

    def block(tp):
        return pl.ds(pl.multiple_of(tp * OWN, OWN), OWN)

    mine = block(j)

    def scatter_third(i):
        here = slice(i * CHUNK, (i + 1) * CHUNK)
        h0 = slice(i * CHUNK, i * CHUNK + half)
        h1 = slice(i * CHUNK + half, (i + 1) * CHUNK)
        for rows_, buffer, k in ((h1, far_l, 2), (h0, far_r, 3), (h0, far_l, 4), (h1, far_r, 5)):
            remote(
                comb.at[next_y, rows_, :], buffer.at[rows_, :], rs_send.at[i, k], rs_recv.at[i, k], up_y
            ).wait_recv()
        r = (
            resid[here, :].astype(F32)
            + comb[y, here, :].astype(F32)
            + (far_l[here, :].astype(F32) + far_r[here, :].astype(F32))
        )
        residual[here, :] = r
        normed[here, mine] = (r * full_gain[:, mine]).astype(BF)
        place = normed.at[here, mine]
        launch(remote(place, place, ag_send.at[i, 0], ag_recv.at[i, 0], up_y))
        launch(remote(place, place, ag_send.at[i, 1], ag_recv.at[i, 1], down_y))
        launch(remote(place, place, pass_send.at[i, 0], pass_recv.at[i, 0], sibling))

    def gather_second(i):
        here = slice(i * CHUNK, (i + 1) * CHUNK)
        h0 = slice(i * CHUNK, i * CHUNK + half)
        h1 = slice(i * CHUNK + half, (i + 1) * CHUNK)
        for k, by, rows_, device in ((0, 3, h0, up_y), (1, 1, h1, down_y)):
            column = block(((y + by) % 4) * 2 + c)
            place = normed.at[here, column]
            remote(place, place, ag_send.at[i, k], ag_recv.at[i, k], device).wait_recv()
            part = normed.at[rows_, column]
            launch(remote(part, part, ag_send.at[i, 2 + k], ag_recv.at[i, 2 + k], device))
            launch(remote(place, place, pass_send.at[i, 1 + k], pass_recv.at[i, 1 + k], sibling))

    def gather_third(i):
        h0 = slice(i * CHUNK, i * CHUNK + half)
        h1 = slice(i * CHUNK + half, (i + 1) * CHUNK)
        column = block(far_y * 2 + c)
        for k, rows_ in ((0, h0), (1, h1)):
            part = normed.at[rows_, column]
            remote(part, part, ag_send.at[i, 2 + k], ag_recv.at[i, 2 + k], sibling).wait_recv()
            launch(remote(part, part, pass_send.at[i, 3 + k], pass_recv.at[i, 3 + k], sibling))

    def gather_last(i):
        here = slice(i * CHUNK, (i + 1) * CHUNK)
        h0 = slice(i * CHUNK, i * CHUNK + half)
        h1 = slice(i * CHUNK + half, (i + 1) * CHUNK)
        for k, by, rows_ in ((0, 0, here), (1, 3, here), (2, 1, here), (3, 2, h0), (4, 2, h1)):
            part = normed.at[rows_, block(((y + by) % 4) * 2 + 1 - c)]
            remote(part, part, pass_send.at[i, k], pass_recv.at[i, k], sibling).wait_recv()
        total_ = jnp.zeros((CHUNK, 128), F32)
        for k in range(WIDTH // 128):
            columns = slice(k * 128, (k + 1) * 128)
            part = normed[here, columns].astype(F32) * (1.0 / full_gain[:, columns])
            total_ = total_ + part * part
        mean = jnp.sum(total_, axis=1, keepdims=True) * (1.0 / WIDTH)
        scale[here, :] = jnp.broadcast_to(lax.rsqrt(mean + EPSILON), (CHUNK, 128))

    locals_ = [local_part(i) for i in range(CHUNKS)]
    for k in range(12, 18):
        loads[k].wait()
    pump_until(3.0)
    receive_state()
    attention(0, locals_[0])
    pump_until(5.0)
    attention(1, locals_[1])
    scatter_first(0)
    pump_until(7.0)
    attention(2, locals_[2])
    pump_until(9.0)
    for time, phase, i in (
        (10.0, scatter_second, 0),
        (10.5, scatter_first, 1),
        (13.0, scatter_third, 0),
        (15.0, scatter_second, 1),
        (15.5, scatter_first, 2),
        (18.0, gather_second, 0),
        (21.0, scatter_third, 1),
        (23.0, scatter_second, 2),
        (25.0, gather_third, 0),
        (28.0, gather_second, 1),
        (31.0, scatter_third, 2),
        (32.0, gather_last, 0),
        (34.0, gather_third, 1),
        (38.0, gather_second, 2),
        (39.0, gather_last, 1),
        (42.0, gather_third, 2),
        (46.0, gather_last, 2),
    ):
        pump_until(time)
        phase(i)
    pump_all(lambda piece: piece[0] == "up")

    def product_of(columns, width):
        wide = scale[...] if width == 128 else jnp.concatenate([scale[...]] * (width // 128), axis=1)
        return (jnp.dot(normed[...], up[:, columns], preferred_element_type=F32) * wide).astype(BF)

    tail = product_of(slice(2 * MAIN, 2 * MAIN + 128), 128).astype(F32)
    gate_tail[...] = pltpu.roll(tail, 64, 1)
    value_tail[...] = pltpu.roll(tail, 32, 1)

    def up_loop(target, offset, low_n, high_n):
        @pl.loop(low_n, high_n)
        def _(n):
            columns = pl.ds(pl.multiple_of(n * 256, 256), 256)
            source = pl.ds(pl.multiple_of(n * 256 + offset, 256), 256)
            target[:, columns] = product_of(source, 256)

    now = max(action[0] for action in actions if action[1] == 0 and action[3][0] == "up")
    pump_until(now + 1.0)
    up_loop(gate, 0, 0, 2)
    pump_until(now + 4.0)
    up_loop(gate, 0, 2, 4)
    edge_out[...] = gate[TOKENS - 16 :, :]
    edge_tail_out[...] = gate_tail[TOKENS - 16 :, :]
    launch(remote(edge_out, edge, edge_send.at[0], edge_recv.at[0], later(1)))
    launch(remote(edge_tail_out, edge_tail, edge_send.at[1], edge_recv.at[1], later(1)))
    pump_until(now + 7.0)
    up_loop(value, MAIN, 0, 2)
    pump_until(now + 10.0)
    up_loop(value, MAIN, 2, 4)
    pump_until(now + 13.0)
    remote(edge_out, edge, edge_send.at[0], edge_recv.at[0], sibling).wait_recv()
    remote(edge_tail_out, edge_tail, edge_send.at[1], edge_recv.at[1], sibling).wait_recv()

    place = lax.broadcasted_iota(jnp.int32, (TOKENS, 1), 0)
    seg = columns_of[:, 0:1]
    last_one, second_one = carried["last"][:, 0:1], carried["second"][:, 0:1]
    before = jnp.where(place == 0, last_one, columns_of[:, 1:2])
    before_two = jnp.where(place == 0, second_one, jnp.where(place == 1, last_one, columns_of[:, 2:3]))
    near_mask = jnp.where(before == seg, 1.0, 0.0)
    far_mask = jnp.where(before_two == seg, 1.0, 0.0)
    wide_near = jnp.broadcast_to(near_mask, (TOKENS, 128)) > 0.5
    wide_far = jnp.broadcast_to(far_mask, (TOKENS, 128)) > 0.5
    at_first = jnp.broadcast_to(place, (TOKENS, 128)) == 0
    at_second = jnp.broadcast_to(place, (TOKENS, 128)) == 1

    def mixed(g, v, tap, previous):
        one = jnp.where(at_first, previous[15:16, :], pltpu.roll(g, 1, 0))
        two = jnp.where(
            at_first, previous[14:15, :], jnp.where(at_second, previous[15:16, :], pltpu.roll(g, 2, 0))
        )
        conv = (
            tap[2:3, :] * g
            + tap[1:2, :] * jnp.where(wide_near, one, 0.0)
            + tap[0:1, :] * jnp.where(wide_far, two, 0.0)
        )
        return (conv * jax.nn.sigmoid(conv) * v).astype(BF)

    lanes = lax.broadcasted_iota(jnp.int32, (TOKENS, 128), 1)
    in_tail = (lanes >= 64) & (lanes < 96)
    tap_tail = jnp.concatenate([jnp.zeros((3, 64), F32), taps[:, MAIN:], jnp.zeros((3, 32), F32)], axis=1)
    hidden_tail[...] = jnp.where(
        in_tail, mixed(gate_tail[...], value_tail[...], tap_tail, edge_tail[...]).astype(F32), 0.0
    ).astype(BF)

    def mix_loop():
        @pl.loop(0, MAIN // 128)
        def _(n):
            columns = pl.ds(pl.multiple_of(n * 128, 128), 128)
            hidden[:, columns] = mixed(
                gate[:, columns].astype(F32),
                value[:, columns].astype(F32),
                taps[:, columns],
                edge[:, columns].astype(F32),
            )

    mix_loop()
    pump_until(now + 16.0)

    def place_of(u):
        return slice(u * UNIT, (u + 1) * UNIT)

    def down_product(p):
        dz, colour, half_ = p
        u = colour * 2 + half_
        target = (z - dz + 4) % 4
        sources = [
            pl.ds(pl.multiple_of((target * 4 + k) * ROWS + u * UNIT, UNIT), UNIT) for k in range(4)
        ]
        main = jnp.concatenate([down[source, :] for source in sources], axis=0)
        rest = jnp.concatenate([up[source, 2 * MAIN :] for source in sources], axis=0)
        result = (
            lax.dot_general(main, hidden[...], NT, preferred_element_type=F32)
            + lax.dot_general(rest, hidden_tail[...], NT, preferred_element_type=F32)
        ).astype(BF)
        for k in range(4):
            dshare[target, k // 2, k % 2, place_of(u), :] = result[k * UNIT : (k + 1) * UNIT]
        launch(dsib_copy(p))

    def dsib_copy(p):
        dz, colour, half_ = p
        u = colour * 2 + half_
        target = (z - dz + 4) % 4
        k = dz * 4 + u
        return remote(
            dshare.at[target, 1 - c, :, place_of(u), :],
            dsib.at[target, :, place_of(u), :],
            dsib_send.at[k],
            dsib_recv.at[k],
            sibling,
        )

    def dcopy(kind, u):
        rows_ = place_of(u)
        source, part, buffer, device = {
            "near_l": (far_y, 0, dnear_l.at[rows_, :], up_y),
            "near_r": (far_y, 1, dnear_r.at[rows_, :], down_y),
            "l1": (next_y, 1, dfar_l.at[1, rows_, :], up_y),
            "r0": (prev_y, 0, dfar_r.at[0, rows_, :], down_y),
            "l0": (next_y, 0, dfar_l.at[0, rows_, :], up_y),
            "r1": (prev_y, 1, dfar_r.at[1, rows_, :], down_y),
        }[kind]
        k = KINDS.index(kind)
        return remote(dcomb.at[source, part, rows_, :], buffer, drs_send.at[k, u], drs_recv.at[k, u], device)

    def down_combine(p):
        dz, colour, half_ = p
        u = colour * 2 + half_
        target = (z - dz + 4) % 4
        rows_ = place_of(u)
        dsib_copy(p).wait_recv()
        for part in range(2):
            dcomb[target, part, rows_, :] = (
                dshare[target, c, part, rows_, :].astype(F32) + dsib[target, part, rows_, :].astype(F32)
            ).astype(BF)

        @pl.when(target == far_y)
        def _():
            dcopy("near_l", u).start()
            dcopy("near_r", u).start()

        @pl.when(target == next_y)
        def _():
            dcopy("l1", u).start()

        @pl.when(target == prev_y)
        def _():
            dcopy("r0", u).start()

    def down_relay(p):
        dz, colour, half_ = p
        u = colour * 2 + half_
        target = (z - dz + 4) % 4
        rows_ = place_of(u)

        @pl.when(target == next_y)
        def _():
            dcopy("near_l", u).wait_recv()
            dcomb[next_y, 0, rows_, :] = (
                dcomb[next_y, 0, rows_, :].astype(F32) + dnear_l[rows_, :].astype(F32)
            ).astype(BF)
            dcopy("l0", u).start()

        @pl.when(target == prev_y)
        def _():
            dcopy("near_r", u).wait_recv()
            dcomb[prev_y, 1, rows_, :] = (
                dcomb[prev_y, 1, rows_, :].astype(F32) + dnear_r[rows_, :].astype(F32)
            ).astype(BF)
            dcopy("r1", u).start()

    def piece_of(item):
        tensor, colour, half_, first, second = item
        return (second if colour == 0 else first, colour, half_)

    completed = {}
    for action in actions:
        if action[1] == 0 and action[3][0] == "down":
            completed[piece_of(action[3])] = action[0]
    for dz_u in [(0, colour, half_) for colour in range(2) for half_ in range(2)]:
        completed.setdefault(dz_u, 0.0)
    order = sorted(completed, key=lambda p: completed[p])
    for index, p in enumerate(order):
        pump_all(lambda item: item[0] == "down" and piece_of(item) == p)
        down_product(p)
        if index >= COMBINE_LAG:
            down_combine(order[index - COMBINE_LAG])
        if index >= RELAY_LAG:
            down_relay(order[index - RELAY_LAG])
    for index in range(len(order), len(order) + RELAY_LAG):
        if index - COMBINE_LAG < len(order):
            down_combine(order[index - COMBINE_LAG])
        down_relay(order[index - RELAY_LAG])
    for kind in ("l1", "r0", "l0", "r1"):
        for u in range(4):
            dcopy(kind, u).wait_recv()
    for part in range(2):
        turned = jnp.transpose(
            dcomb[y, part].astype(F32) + (dfar_l[part].astype(F32) + dfar_r[part].astype(F32))
        )
        here = slice(part * ROWS, (part + 1) * ROWS)
        out[:, here] = (residual[:, here] + turned).astype(BF)

    for kind in KINDS:
        for u in range(4):
            dcopy(kind, u).wait_send()
    for copy in waiting:
        copy.wait_send()


def body(
    resid, query, keys, values, out_gate, in_gate, forget, doc_ids, head_gain, w_out, ffn_gain,
    w_gate, w_value, conv_taps, w_down,
):
    hbm = pl.BlockSpec(memory_space=pl.ANY)
    dma = pltpu.SemaphoreType.DMA
    turned = [pltpu.VMEM((HEADS, TOKENS), BF)] * 4
    scratch = [
        pltpu.VMEM((TOKENS, OWN), BF),
        *turned,
        pltpu.VMEM((2, TOKENS), F32),
        pltpu.VMEM((2, TOKENS), F32),
        pltpu.VMEM((1, TOKENS), jnp.int32),
        pltpu.VMEM((1, HEADS), F32),
        pltpu.VMEM((HEADS, WIDTH), BF),
        pltpu.VMEM((1, WIDTH), F32),
        pltpu.VMEM((3, MAIN + 32), F32),
        pltpu.VMEM((ROWS, MAIN + 32), BF),
        pltpu.VMEM((ROWS, MAIN + 32), BF),
        pltpu.VMEM((ROWS, MAIN + 32), BF),
        pltpu.VMEM((TOKENS, 128), F32),
        pltpu.VMEM((WIDTH, 2 * MAIN + 128), BF),
        pltpu.VMEM((WIDTH, MAIN), BF),
        pltpu.VMEM((TOKENS, WIDTH), BF),
        pltpu.VMEM((2, 4, TOKENS, OWN), BF),
        pltpu.VMEM((4, TOKENS, OWN), BF),
        pltpu.VMEM((4, TOKENS, OWN), BF),
        pltpu.VMEM((TOKENS // 2, OWN), BF),
        pltpu.VMEM((TOKENS // 2, OWN), BF),
        pltpu.VMEM((TOKENS, OWN), BF),
        pltpu.VMEM((TOKENS, OWN), BF),
        pltpu.VMEM((TOKENS, OWN), F32),
        pltpu.VMEM((TOKENS, MAIN), BF),
        pltpu.VMEM((TOKENS, MAIN), BF),
        pltpu.VMEM((TOKENS, 128), F32),
        pltpu.VMEM((TOKENS, 128), F32),
        pltpu.VMEM((TOKENS, MAIN), BF),
        pltpu.VMEM((TOKENS, 128), BF),
        pltpu.VMEM((16, MAIN), BF),
        pltpu.VMEM((16, 128), F32),
        pltpu.VMEM((16, MAIN), BF),
        pltpu.VMEM((16, 128), F32),
        pltpu.VMEM((TOKENS, 128), F32),
        pltpu.VMEM((DH, HEADS), BF),
        pltpu.VMEM((8, HEADS), F32),
        pltpu.VMEM((4, DH, HEADS), BF),
        pltpu.VMEM((4, 8, HEADS), F32),
        pltpu.VMEM((4, 2, 2, ROWS, TOKENS), BF),
        pltpu.VMEM((4, 2, ROWS, TOKENS), BF),
        pltpu.VMEM((4, 2, ROWS, TOKENS), BF),
        pltpu.VMEM((ROWS, TOKENS), BF),
        pltpu.VMEM((ROWS, TOKENS), BF),
        pltpu.VMEM((2, ROWS, TOKENS), BF),
        pltpu.VMEM((2, ROWS, TOKENS), BF),
        dma((18,)),
        dma((64,)),
        dma((64,)),
        dma((64,)),
        dma((64,)),
        dma((4,)),
        dma((4,)),
        dma((4,)),
        dma((4,)),
        dma((2,)),
        dma((2,)),
        dma((CHUNKS,)),
        dma((CHUNKS,)),
        dma((CHUNKS, 6)),
        dma((CHUNKS, 6)),
        dma((CHUNKS, 4)),
        dma((CHUNKS, 4)),
        dma((CHUNKS, 5)),
        dma((CHUNKS, 5)),
        dma((16,)),
        dma((16,)),
        dma((6, 4)),
        dma((6, 4)),
    ]
    return pl.pallas_call(
        layer_kernel,
        in_specs=[hbm] * 15,
        out_specs=pl.BlockSpec(memory_space=pltpu.VMEM),
        out_shape=jax.ShapeDtypeStruct((TOKENS, OWN), BF),
        scratch_shapes=scratch,
        compiler_params=pltpu.CompilerParams(
            collective_id=0, has_side_effects=True, vmem_limit_bytes=67043328
        ),
        name="layer",
    )(
        resid, query.T, keys.T, values.T, out_gate.T, in_gate, forget, doc_ids[None], head_gain[None], w_out,
        ffn_gain[None], w_gate, w_value, conv_taps, w_down.T,
    )


def solution(mesh):
    placed = (
        P("sp", "tp"),
        P("sp", "tp"),
        P("sp", "tp"),
        P("sp", "tp"),
        P("sp", "tp"),
        P("tp", "sp"),
        P("tp", "sp"),
        P("sp"),
        P("tp"),
        P("tp", None),
        P(),
        P("sp", "tp"),
        P("sp", "tp"),
        P(None, "tp"),
        P("tp", "sp"),
    )
    return jax.shard_map(body, mesh=mesh, in_specs=placed, out_specs=P("sp", "tp"), check_vma=False)
```

time: 194 us -> 147 us (0.76)
  Pallas kernels: 175 us -> 141 us
  local copies, waits for them, and re-layouts: 12.4 us -> 3.2 us
  other arithmetic: 3.62 us -> 0 us
    pallas_call x1, Pallas kernels: 175 us -> 141 us  [body(): pl.pallas_call(layer_kernel, in_specs=[hbm] * 15, out_specs=pl.BlockSpec(...]
    unnamed x17 -> x1, local copies, waits for them, and re-layouts: 5.67 us -> 1.94 us
    slice x15 -> x0, local copies, waits for them, and re-layouts: 2.46 us -> none  [the longest x1 0.8 us: body(): turned[:, MAIN:]]
where the time goes in v1:
time: 147 us; the launch traced here: 145 us
  Pallas kernels  141 us (96%)
  local copies, waits for them, and re-layouts  3.2 us (2%)
    pallas_call x1, Pallas kernels, body(): pl.pallas_call(layer_kernel, in_specs=[hbm] * 15, out_specs=pl.BlockSpec(...  141 us

profile of v1, /device:TPU:16, one launch (start us, length us, event | category | flops | bytes accessed | tf_op | source)
XLA Modules:
  0.0 144.6 jit_solution(17997149926957515425)
XLA Ops:
  0.0 1.3 broadcast_in_dim.9.docs_hbm
  1.3 141.4 %layer.1 = bf16[768,384]{1,0:T(8,128)(2,1)} custom-call(bf16[768,384]{1,0:T(8,128)(2,1)} %resid_hbm.1, bf16[192,768]{1,0:T(8,128)(2,1)} %bitcast.8, bf16[192,768]{1,0:T(8,128)(2,1)} %bitcast.9, bf16[192,768]{1,0:T(8,128)(2,1)} %bitcast.10, bf16[192,768]{1,0:T(8,128)(2,1)} %bitcast.11, f32[2,768]{1,0:T(2,128)} %in_gate_hbm.1, f32[2,768]{1,0:T(2,128)} %forget_hbm.1, ...), custom_call_target="tpu_custom_call" | custom-call | tf_op jit(solution)/shard_map/layer/pallas_call | solution.py:779
  142.7 1.9 %copy.17 = bf16[768,384]{1,0:T(8,128)(2,1)} copy(bf16[768,384]{1,0:T(8,128)(2,1)} %layer.1) | data formatting | bytes 1179648

commit v2 on v1

--- a/solution.py
+++ b/solution.py
@@ -21,8 +21,8 @@
 CHUNKS = TOKENS // CHUNK
 UNIT = 48
 KINDS = ("near_l", "near_r", "l1", "r0", "l0", "r1")
-COMBINE_LAG = 2
-RELAY_LAG = 6
+COMBINE_LAG = 1
+RELAY_LAG = 3
 BF = jnp.bfloat16
 F32 = jnp.float32
 MESH = pl.DeviceIdType.MESH
@@ -30,7 +30,7 @@
 TN = (((0,), (0,)), ((), ()))
 
 RATES = {"up": 4.6, "down": 2.2}
-HOP = 2.2
+HOP = 4.5
 LEAD = 9.0
 LATE = {3: 0, 1: 1, 2: 2, 0: 3}
 
@@ -119,7 +119,7 @@
     load_sem, send_up, recv_up, send_down, recv_down,
     state_send, state_recv, meta_send, meta_recv, edge_send, edge_recv,
     sib_send, sib_recv, rs_send, rs_recv, ag_send, ag_recv, pass_send, pass_recv,
-    dsib_send, dsib_recv, drs_send, drs_recv,
+    dsib_send, dsib_recv, drs_send, drs_recv, result, out_sem,
 ):
     s = lax.axis_index("sp")
     j = lax.axis_index("tp")
@@ -189,6 +189,10 @@
         copy.start()
         waiting.append(copy)
 
+    def drain(keep):
+        while len(waiting) > keep:
+            waiting.pop(0).wait_send()
+
     gathered = {"up": (up, send_up, recv_up), "down": (down, send_down, recv_down)}
 
     def origin(piece):
@@ -243,7 +247,7 @@
     for k in range(10):
         if 1 << k < TOKENS:
             cumul = cumul + jnp.where(token >= 1 << k, pltpu.roll(cumul, 1 << k, 1), 0.0)
-    seg_row = docs[...].astype(F32)
+    seg_row = jnp.concatenate([docs[k : k + 1, :] for k in range(6)], axis=1).astype(F32)
     g_rows = [in_gate[h : h + 1, :] - cumul[h : h + 1, :] for h in range(2)]
     last_seg = seg_row[:, TOKENS - 1 : TOKENS]
     second_seg = seg_row[:, TOKENS - 2 : TOKENS - 1]
@@ -468,26 +472,28 @@
     attention(2, locals_[2])
     pump_until(9.0)
     for time, phase, i in (
-        (10.0, scatter_second, 0),
-        (10.5, scatter_first, 1),
-        (13.0, scatter_third, 0),
-        (15.0, scatter_second, 1),
-        (15.5, scatter_first, 2),
-        (18.0, gather_second, 0),
-        (21.0, scatter_third, 1),
-        (23.0, scatter_second, 2),
-        (25.0, gather_third, 0),
-        (28.0, gather_second, 1),
-        (31.0, scatter_third, 2),
-        (32.0, gather_last, 0),
-        (34.0, gather_third, 1),
-        (38.0, gather_second, 2),
-        (39.0, gather_last, 1),
-        (42.0, gather_third, 2),
-        (46.0, gather_last, 2),
+        (11.0, scatter_second, 0),
+        (14.0, scatter_first, 1),
+        (14.5, scatter_third, 0),
+        (18.0, scatter_second, 1),
+        (20.0, scatter_first, 2),
+        (21.0, gather_second, 0),
+        (25.0, scatter_third, 1),
+        (27.0, scatter_second, 2),
+        (29.0, gather_third, 0),
+        (33.0, gather_second, 1),
+        (37.0, scatter_third, 2),
+        (39.0, gather_last, 0),
+        (40.0, gather_third, 1),
+        (42.0, gather_second, 2),
+        (47.0, gather_last, 1),
+        (48.0, gather_third, 2),
+        (51.0, gather_last, 2),
     ):
         pump_until(time)
         phase(i)
+    pump_until(56.0)
+    drain(40)
     pump_all(lambda piece: piece[0] == "up")
 
     def product_of(columns, width):
@@ -565,27 +571,31 @@
             )
 
     mix_loop()
-    pump_until(now + 16.0)
+    pump_until(now + 15.5)
 
     def place_of(u):
         return slice(u * UNIT, (u + 1) * UNIT)
 
-    def down_product(p):
-        dz, colour, half_ = p
-        u = colour * 2 + half_
-        target = (z - dz + 4) % 4
-        sources = [
-            pl.ds(pl.multiple_of((target * 4 + k) * ROWS + u * UNIT, UNIT), UNIT) for k in range(4)
-        ]
+    def down_product(ps):
+        sources = []
+        for dz, colour, half_ in ps:
+            target = (z - dz + 4) % 4
+            for k in range(4):
+                row = (target * 4 + k) * ROWS + (colour * 2 + half_) * UNIT
+                sources.append(pl.ds(pl.multiple_of(row, UNIT), UNIT))
         main = jnp.concatenate([down[source, :] for source in sources], axis=0)
         rest = jnp.concatenate([up[source, 2 * MAIN :] for source in sources], axis=0)
         result = (
             lax.dot_general(main, hidden[...], NT, preferred_element_type=F32)
             + lax.dot_general(rest, hidden_tail[...], NT, preferred_element_type=F32)
         ).astype(BF)
-        for k in range(4):
-            dshare[target, k // 2, k % 2, place_of(u), :] = result[k * UNIT : (k + 1) * UNIT]
-        launch(dsib_copy(p))
+        for index, p in enumerate(ps):
+            dz, colour, half_ = p
+            target = (z - dz + 4) % 4
+            for k in range(4):
+                row = (index * 4 + k) * UNIT
+                dshare[target, k // 2, k % 2, place_of(colour * 2 + half_), :] = result[row : row + UNIT]
+            launch(dsib_copy(p))
 
     def dsib_copy(p):
         dz, colour, half_ = p
@@ -669,33 +679,43 @@
             completed[piece_of(action[3])] = action[0]
     for dz_u in [(0, colour, half_) for colour in range(2) for half_ in range(2)]:
         completed.setdefault(dz_u, 0.0)
-    order = sorted(completed, key=lambda p: completed[p])
-    for index, p in enumerate(order):
-        pump_all(lambda item: item[0] == "down" and piece_of(item) == p)
-        down_product(p)
-        if index >= COMBINE_LAG:
-            down_combine(order[index - COMBINE_LAG])
+    order = sorted(completed, key=lambda p: (completed[p], p))
+    groups = [order[k : k + 2] for k in range(0, 16, 2)]
+    start_time = now + 15.5
+    for index in range(len(groups) + RELAY_LAG):
+        if index < len(groups):
+            ps = groups[index]
+            pump_until(start_time + 2.0 * index)
+            pump_all(lambda item: item[0] == "down" and piece_of(item) in ps)
+            down_product(ps)
+        if 0 <= index - COMBINE_LAG < len(groups):
+            for p in groups[index - COMBINE_LAG]:
+                down_combine(p)
         if index >= RELAY_LAG:
-            down_relay(order[index - RELAY_LAG])
-    for index in range(len(order), len(order) + RELAY_LAG):
-        if index - COMBINE_LAG < len(order):
-            down_combine(order[index - COMBINE_LAG])
-        down_relay(order[index - RELAY_LAG])
+            for p in groups[index - RELAY_LAG]:
+                down_relay(p)
+        if index == len(groups):
+            drain(8)
     for kind in ("l1", "r0", "l0", "r1"):
         for u in range(4):
             dcopy(kind, u).wait_recv()
-    for part in range(2):
-        turned = jnp.transpose(
-            dcomb[y, part].astype(F32) + (dfar_l[part].astype(F32) + dfar_r[part].astype(F32))
-        )
-        here = slice(part * ROWS, (part + 1) * ROWS)
-        out[:, here] = (residual[:, here] + turned).astype(BF)
+    stores = []
+    for i in range(CHUNKS):
+        here = slice(i * CHUNK, (i + 1) * CHUNK)
+        summed = [
+            dcomb[y, part, :, here].astype(F32) + (dfar_l[part, :, here].astype(F32) + dfar_r[part, :, here].astype(F32))
+            for part in range(2)
+        ]
+        result[here, :] = (residual[here, :] + jnp.transpose(jnp.concatenate(summed, axis=0))).astype(BF)
+        stores.append(pltpu.make_async_copy(result.at[here, :], out.at[here, :], out_sem.at[i]))
+        stores[i].start()
 
     for kind in KINDS:
         for u in range(4):
             dcopy(kind, u).wait_send()
-    for copy in waiting:
-        copy.wait_send()
+    drain(0)
+    for store in stores:
+        store.wait()
 
 
 def body(
@@ -710,7 +730,7 @@
         *turned,
         pltpu.VMEM((2, TOKENS), F32),
         pltpu.VMEM((2, TOKENS), F32),
-        pltpu.VMEM((1, TOKENS), jnp.int32),
+        pltpu.VMEM((6, 128), jnp.int32),
         pltpu.VMEM((1, HEADS), F32),
         pltpu.VMEM((HEADS, WIDTH), BF),
         pltpu.VMEM((1, WIDTH), F32),
@@ -775,19 +795,21 @@
         dma((16,)),
         dma((6, 4)),
         dma((6, 4)),
+        pltpu.VMEM((TOKENS, OWN), BF),
+        dma((CHUNKS,)),
     ]
     return pl.pallas_call(
         layer_kernel,
         in_specs=[hbm] * 15,
-        out_specs=pl.BlockSpec(memory_space=pltpu.VMEM),
+        out_specs=hbm,
         out_shape=jax.ShapeDtypeStruct((TOKENS, OWN), BF),
         scratch_shapes=scratch,
         compiler_params=pltpu.CompilerParams(
-            collective_id=0, has_side_effects=True, vmem_limit_bytes=67043328
+            collective_id=0, has_side_effects=True, vmem_limit_bytes=63000000
         ),
         name="layer",
     )(
-        resid, query.T, keys.T, values.T, out_gate.T, in_gate, forget, doc_ids[None], head_gain[None], w_out,
+        resid, query.T, keys.T, values.T, out_gate.T, in_gate, forget, doc_ids.reshape(6, 128), head_gain[None], w_out,
         ffn_gain[None], w_gate, w_value, conv_taps, w_down.T,
     )
 

time: 147 us -> 142 us (0.966); the launches traced: 145 us -> 141 us
  Pallas kernels: 141 us -> 139 us
    pallas_call x1, Pallas kernels: 141 us -> 139 us  [body(): pl.pallas_call(layer_kernel, in_specs=[hbm] * 15, out_specs=hbm, out_shap...]
where the time goes in v2:
time: 142 us; the launch traced here: 141 us
  Pallas kernels  139 us (98%)
  local copies, waits for them, and re-layouts  1.94 us (1%)
    pallas_call x1, Pallas kernels, body(): pl.pallas_call(layer_kernel, in_specs=[hbm] * 15, out_specs=hbm, out_shap...  139 us

profile of v2, /device:TPU:16, one launch (start us, length us, event | category | flops | bytes accessed | tf_op | source)
XLA Modules:
  0.0 141.2 jit_solution(10797015084252742634)
XLA Ops:
  0.0 139.3 %layer.1 = bf16[768,384]{1,0:T(8,128)(2,1)} custom-call(bf16[768,384]{1,0:T(8,128)(2,1)} %resid_hbm.1, bf16[192,768]{1,0:T(8,128)(2,1)} %bitcast.9, bf16[192,768]{1,0:T(8,128)(2,1)} %bitcast.10, bf16[192,768]{1,0:T(8,128)(2,1)} %bitcast.11, bf16[192,768]{1,0:T(8,128)(2,1)} %bitcast.12, f32[2,768]{1,0:T(2,128)} %in_gate_hbm.1, f32[2,768]{1,0:T(2,128)} %forget_hbm.1, ...), custom_call_target="tpu_custom_call" | custom-call | tf_op jit(solution)/shard_map/layer/pallas_call | solution.py:801
  139.3 1.9 %copy.17 = bf16[768,384]{1,0:T(8,128)(2,1)} copy(bf16[768,384]{1,0:T(8,128)(2,1)} %layer.1) | data formatting | bytes 1179648

commit v3 on v2

--- a/solution.py
+++ b/solution.py
@@ -17,12 +17,13 @@
 OWN = 384
 HEADS = 192
 MAIN = 1024
+LAST = slice(2 * MAIN, 2 * MAIN + 128)
 CHUNK = 256
 CHUNKS = TOKENS // CHUNK
 UNIT = 48
 KINDS = ("near_l", "near_r", "l1", "r0", "l0", "r1")
 COMBINE_LAG = 1
-RELAY_LAG = 3
+RELAY_LAG = 4
 BF = jnp.bfloat16
 F32 = jnp.float32
 MESH = pl.DeviceIdType.MESH
@@ -30,9 +31,13 @@
 TN = (((0,), (0,)), ((), ()))
 
 RATES = {"up": 4.6, "down": 2.2}
-HOP = 4.5
+HOP = 4.0
 LEAD = 9.0
-LATE = {3: 0, 1: 1, 2: 2, 0: 3}
+LATE = (0, 1, 2, 4)
+LATE_ROW = ((3, 3, 3, 1), (1, 3, 6, 4))
+HELD = {("x", 1): 3.4, ("x", -1): 1.1, ("z", 1): 2.3, ("z", -1): 0.0}
+EARLY = {0: 0, 1: 1, 3: 2, 2: 3}
+GROUP = 4 * ROWS
 
 
 def axes(colour):
@@ -65,17 +70,15 @@
 def urgency(start):
     tensor, colour, half, first, second = landing(start)
     if tensor == "up":
-        return (0, -depth(start), half)
-    if second == 0:
-        return (1, 0, -depth(start))
-    if colour == 0:
-        return (1, 1, 0 if start[2] == (1 if half == 0 else -1) else 1, -depth(start))
-    return (1, 1, LATE[first], -depth(start))
+        return (0, EARLY[second if colour == 0 else first] - depth(start), half)
+    row = second if colour == 0 else first
+    row = row if half == 0 else -row % 4
+    return (1, LATE[colour * 2 + half] + LATE_ROW[colour][row] - 2 * depth(start) - (6 if second == 0 else 0))
 
 
 def gather_plan():
-    ready = {(axis, way): [] for axis in "xz" for way in (1, -1)}
-    busy = dict.fromkeys(ready, 0.0)
+    ready = {link: [] for link in HELD}
+    busy = dict(HELD)
     arrivals, actions, count, now = [], [], 0, 0.0
 
     def add(time, piece):
@@ -96,7 +99,7 @@
                 count += 1
                 heapq.heappush(arrivals, (busy[link] + HOP, count, landing(start)))
                 actions.append((max(since, now - LEAD), 1, count, start))
-        times = [busy[link] for link in ready if ready[link]] + [entry[0] for entry in arrivals[:1]]
+        times = [busy[link] for link in ready if ready[link] and busy[link] > now] + [entry[0] for entry in arrivals[:1]]
         if not times:
             return sorted(actions, key=lambda action: action[:3])
         now = min(times)
@@ -113,7 +116,7 @@
     resid, query, keys, values, out_gate, in_gate, forget, docs, head_gain, w_out, full_gain, taps,
     stage_gate, stage_value, stage_down, columns_of,
     up, down, normed, share, sib, comb, near_l, near_r, far_l, far_r, residual,
-    gate, value, gate_tail, value_tail, hidden, hidden_tail, edge, edge_tail, edge_out, edge_tail_out,
+    acc, gate, value, hidden_tail, edge, edge_tail, edge_out, edge_tail_out, gate_head,
     scale, state_out, meta_out, states, metas,
     dshare, dsib, dcomb, dnear_l, dnear_r, dfar_l, dfar_r,
     load_sem, send_up, recv_up, send_down, recv_down,
@@ -183,15 +186,11 @@
             src_ref=src, dst_ref=dst, send_sem=send, recv_sem=recv, device_id=device, device_id_type=MESH
         )
 
-    waiting = []
-
     def launch(copy):
         copy.start()
-        waiting.append(copy)
-
-    def drain(keep):
-        while len(waiting) > keep:
-            waiting.pop(0).wait_send()
+
+    def sent(ref, sem):
+        remote(ref, ref, sem.at[0], sem.at[0], sibling).wait_send()
 
     gathered = {"up": (up, send_up, recv_up), "down": (down, send_down, recv_down)}
 
@@ -210,7 +209,7 @@
         buffer, send, recv = gathered[piece[0]]
         place = buffer.at[origin(piece), :]
         k = slot(landing(start))
-        launch(remote(place, place, send.at[k], recv.at[k], (chip_x if axis == "x" else chip_z)(direction)))
+        launch(remote(place, place, send.at[0], recv.at[k], (chip_x if axis == "x" else chip_z)(direction)))
 
     actions = gather_plan()
     position = [0]
@@ -224,8 +223,13 @@
         else:
             buffer, send, recv = gathered[item[0]]
             place = buffer.at[origin(item), :]
-            remote(place, place, send.at[slot(item)], recv.at[slot(item)], sibling).wait_recv()
+            remote(place, place, send.at[0], recv.at[slot(item)], sibling).wait_recv()
             arrived.add(item)
+
+    middle = [0.0]
+
+    def dz_of(piece):
+        return piece[4] if piece[1] == 0 else piece[3]
 
     def pump_until(time):
         while position[0] < len(actions) and actions[position[0]][0] <= time:
@@ -292,8 +296,8 @@
 
     pl.semaphore_wait(barrier, len(partners))
     for by in range(1, 5):
-        launch(remote(meta_out, metas.at[by - 1], meta_send.at[by - 1], meta_recv.at[by - 1], later(by)))
-        launch(remote(state_out, states.at[by - 1], state_send.at[by - 1], state_recv.at[by - 1], later(by)))
+        launch(remote(meta_out, metas.at[by - 1], meta_send.at[0], meta_recv.at[by - 1], later(by)))
+        launch(remote(state_out, states.at[by - 1], state_send.at[0], state_recv.at[by - 1], later(by)))
     pump_until(0.0)
 
     def local_part(i):
@@ -317,8 +321,8 @@
 
     def receive_state():
         for by in range(1, 5):
-            remote(meta_out, metas.at[by - 1], meta_send.at[by - 1], meta_recv.at[by - 1], sibling).wait_recv()
-            remote(state_out, states.at[by - 1], state_send.at[by - 1], state_recv.at[by - 1], sibling).wait_recv()
+            remote(meta_out, metas.at[by - 1], meta_send.at[0], meta_recv.at[by - 1], sibling).wait_recv()
+            remote(state_out, states.at[by - 1], state_send.at[0], state_recv.at[by - 1], sibling).wait_recv()
         last_prev = jnp.where(s >= 1, metas[0, 2:3, :], -1.0)
         passed = jnp.zeros((1, HEADS), F32)
         logs = []
@@ -357,7 +361,7 @@
             share[k % 2, k // 2, here, :] = jnp.dot(
                 mix, w_out[:, k * OWN : (k + 1) * OWN], preferred_element_type=F32
             ).astype(BF)
-        launch(remote(share.at[1 - c, :, here, :], sib.at[:, here, :], sib_send.at[i], sib_recv.at[i], sibling))
+        launch(remote(share.at[1 - c, :, here, :], sib.at[:, here, :], sib_send.at[0], sib_recv.at[i], sibling))
 
     up_y, down_y = chip_y(1), chip_y(-1)
     next_y, prev_y, far_y = (y + 1) % 4, (y + 3) % 4, (y + 2) % 4
@@ -369,16 +373,16 @@
         h1 = slice(i * CHUNK + half, (i + 1) * CHUNK)
         n = slice(i * half, (i + 1) * half)
         remote(
-            share.at[1 - c, :, here, :], sib.at[:, here, :], sib_send.at[i], sib_recv.at[i], sibling
+            share.at[1 - c, :, here, :], sib.at[:, here, :], sib_send.at[0], sib_recv.at[i], sibling
         ).wait_recv()
         for k in range(4):
             comb[k, here, :] = (
                 share[c, k, here, :].astype(F32) + sib[k, here, :].astype(F32)
             ).astype(BF)
-        launch(remote(comb.at[far_y, h0, :], near_l.at[n, :], rs_send.at[i, 0], rs_recv.at[i, 0], up_y))
-        launch(remote(comb.at[far_y, h1, :], near_r.at[n, :], rs_send.at[i, 1], rs_recv.at[i, 1], down_y))
-        launch(remote(comb.at[next_y, h1, :], far_l.at[h1, :], rs_send.at[i, 2], rs_recv.at[i, 2], up_y))
-        launch(remote(comb.at[prev_y, h0, :], far_r.at[h0, :], rs_send.at[i, 3], rs_recv.at[i, 3], down_y))
+        launch(remote(comb.at[far_y, h0, :], near_l.at[n, :], rs_send.at[0], rs_recv.at[i, 0], up_y))
+        launch(remote(comb.at[far_y, h1, :], near_r.at[n, :], rs_send.at[0], rs_recv.at[i, 1], down_y))
+        launch(remote(comb.at[next_y, h1, :], far_l.at[h1, :], rs_send.at[0], rs_recv.at[i, 2], up_y))
+        launch(remote(comb.at[prev_y, h0, :], far_r.at[h0, :], rs_send.at[0], rs_recv.at[i, 3], down_y))
 
     def scatter_second(i):
         h0 = slice(i * CHUNK, i * CHUNK + half)
@@ -388,13 +392,14 @@
             (next_y, h0, near_l, far_l, 0, up_y),
             (prev_y, h1, near_r, far_r, 1, down_y),
         ):
-            remote(comb.at[far_y, rows_, :], buffer.at[n, :], rs_send.at[i, k], rs_recv.at[i, k], device).wait_recv()
+            remote(comb.at[far_y, rows_, :], buffer.at[n, :], rs_send.at[0], rs_recv.at[i, k], device).wait_recv()
             comb[place, rows_, :] = (
                 comb[place, rows_, :].astype(F32) + buffer[n, :].astype(F32)
             ).astype(BF)
+            pump_until(middle[0])
             launch(
                 remote(
-                    comb.at[place, rows_, :], far.at[rows_, :], rs_send.at[i, 4 + k], rs_recv.at[i, 4 + k], device
+                    comb.at[place, rows_, :], far.at[rows_, :], rs_send.at[0], rs_recv.at[i, 4 + k], device
                 )
             )
 
@@ -408,8 +413,9 @@
         h0 = slice(i * CHUNK, i * CHUNK + half)
         h1 = slice(i * CHUNK + half, (i + 1) * CHUNK)
         for rows_, buffer, k in ((h1, far_l, 2), (h0, far_r, 3), (h0, far_l, 4), (h1, far_r, 5)):
+            pump_until(middle[0])
             remote(
-                comb.at[next_y, rows_, :], buffer.at[rows_, :], rs_send.at[i, k], rs_recv.at[i, k], up_y
+                comb.at[next_y, rows_, :], buffer.at[rows_, :], rs_send.at[0], rs_recv.at[i, k], up_y
             ).wait_recv()
         r = (
             resid[here, :].astype(F32)
@@ -419,9 +425,9 @@
         residual[here, :] = r
         normed[here, mine] = (r * full_gain[:, mine]).astype(BF)
         place = normed.at[here, mine]
-        launch(remote(place, place, ag_send.at[i, 0], ag_recv.at[i, 0], up_y))
-        launch(remote(place, place, ag_send.at[i, 1], ag_recv.at[i, 1], down_y))
-        launch(remote(place, place, pass_send.at[i, 0], pass_recv.at[i, 0], sibling))
+        launch(remote(place, place, ag_send.at[0], ag_recv.at[i, 0], up_y))
+        launch(remote(place, place, ag_send.at[0], ag_recv.at[i, 1], down_y))
+        launch(remote(place, place, pass_send.at[0], pass_recv.at[i, 0], sibling))
 
     def gather_second(i):
         here = slice(i * CHUNK, (i + 1) * CHUNK)
@@ -430,10 +436,11 @@
         for k, by, rows_, device in ((0, 3, h0, up_y), (1, 1, h1, down_y)):
             column = block(((y + by) % 4) * 2 + c)
             place = normed.at[here, column]
-            remote(place, place, ag_send.at[i, k], ag_recv.at[i, k], device).wait_recv()
+            remote(place, place, ag_send.at[0], ag_recv.at[i, k], device).wait_recv()
             part = normed.at[rows_, column]
-            launch(remote(part, part, ag_send.at[i, 2 + k], ag_recv.at[i, 2 + k], device))
-            launch(remote(place, place, pass_send.at[i, 1 + k], pass_recv.at[i, 1 + k], sibling))
+            launch(remote(part, part, ag_send.at[0], ag_recv.at[i, 2 + k], device))
+            launch(remote(place, place, pass_send.at[0], pass_recv.at[i, 1 + k], sibling))
+            pump_until(middle[0])
 
     def gather_third(i):
         h0 = slice(i * CHUNK, i * CHUNK + half)
@@ -441,8 +448,9 @@
         column = block(far_y * 2 + c)
         for k, rows_ in ((0, h0), (1, h1)):
             part = normed.at[rows_, column]
-            remote(part, part, ag_send.at[i, 2 + k], ag_recv.at[i, 2 + k], sibling).wait_recv()
-            launch(remote(part, part, pass_send.at[i, 3 + k], pass_recv.at[i, 3 + k], sibling))
+            remote(part, part, ag_send.at[0], ag_recv.at[i, 2 + k], sibling).wait_recv()
+            launch(remote(part, part, pass_send.at[0], pass_recv.at[i, 3 + k], sibling))
+            pump_until(middle[0])
 
     def gather_last(i):
         here = slice(i * CHUNK, (i + 1) * CHUNK)
@@ -450,7 +458,7 @@
         h1 = slice(i * CHUNK + half, (i + 1) * CHUNK)
         for k, by, rows_ in ((0, 0, here), (1, 3, here), (2, 1, here), (3, 2, h0), (4, 2, h1)):
             part = normed.at[rows_, block(((y + by) % 4) * 2 + 1 - c)]
-            remote(part, part, pass_send.at[i, k], pass_recv.at[i, k], sibling).wait_recv()
+            remote(part, part, pass_send.at[0], pass_recv.at[i, k], sibling).wait_recv()
         total_ = jnp.zeros((CHUNK, 128), F32)
         for k in range(WIDTH // 128):
             columns = slice(k * 128, (k + 1) * 128)
@@ -471,107 +479,141 @@
     pump_until(7.0)
     attention(2, locals_[2])
     pump_until(9.0)
-    for time, phase, i in (
-        (11.0, scatter_second, 0),
-        (14.0, scatter_first, 1),
-        (14.5, scatter_third, 0),
-        (18.0, scatter_second, 1),
-        (20.0, scatter_first, 2),
-        (21.0, gather_second, 0),
-        (25.0, scatter_third, 1),
-        (27.0, scatter_second, 2),
-        (29.0, gather_third, 0),
-        (33.0, gather_second, 1),
-        (37.0, scatter_third, 2),
-        (39.0, gather_last, 0),
-        (40.0, gather_third, 1),
-        (42.0, gather_second, 2),
-        (47.0, gather_last, 1),
-        (48.0, gather_third, 2),
-        (51.0, gather_last, 2),
+    for time, middle[0], phase, i in (
+        (11.0, 13.5, scatter_second, 0),
+        (15.0, 15.0, scatter_first, 1),
+        (15.5, 18.0, scatter_third, 0),
+        (19.5, 21.0, scatter_second, 1),
+        (22.0, 22.0, scatter_first, 2),
+        (22.5, 25.0, gather_second, 0),
+        (27.0, 28.0, scatter_third, 1),
+        (29.5, 30.5, scatter_second, 2),
+        (31.5, 33.5, gather_third, 0),
+        (35.5, 37.5, gather_second, 1),
+        (39.5, 41.0, scatter_third, 2),
+        (42.0, 42.0, gather_last, 0),
+        (42.5, 43.0, gather_third, 1),
+        (44.0, 46.5, gather_second, 2),
+        (49.0, 49.0, gather_last, 1),
+        (49.5, 50.5, gather_third, 2),
+        (52.0, 52.0, gather_last, 2),
     ):
         pump_until(time)
         phase(i)
-    pump_until(56.0)
-    drain(40)
-    pump_all(lambda piece: piece[0] == "up")
-
-    def product_of(columns, width):
-        wide = scale[...] if width == 128 else jnp.concatenate([scale[...]] * (width // 128), axis=1)
-        return (jnp.dot(normed[...], up[:, columns], preferred_element_type=F32) * wide).astype(BF)
-
-    tail = product_of(slice(2 * MAIN, 2 * MAIN + 128), 128).astype(F32)
-    gate_tail[...] = pltpu.roll(tail, 64, 1)
-    value_tail[...] = pltpu.roll(tail, 32, 1)
-
-    def up_loop(target, offset, low_n, high_n):
+
+    def group_product(dz, columns):
+        inner = pl.ds(pl.multiple_of(((z - dz + 4) % 4) * GROUP, GROUP), GROUP)
+        return jnp.dot(normed[:, inner], up[inner, columns], preferred_element_type=F32)
+
+    def group_loop(dzs, first, low_n, high_n):
+        def add(columns):
+            part = group_product(dzs[0], columns)
+            for dz in dzs[1:]:
+                part = part + group_product(dz, columns)
+            acc[:, columns] = part if first else acc[:, columns] + part
+
         @pl.loop(low_n, high_n)
+        def _(n):
+            add(pl.ds(pl.multiple_of(n * 256, 256), 256))
+
+        if high_n == 8:
+            add(LAST)
+
+    def final_loop(dz, target, offset):
+        @pl.loop(0, 4)
         def _(n):
             columns = pl.ds(pl.multiple_of(n * 256, 256), 256)
             source = pl.ds(pl.multiple_of(n * 256 + offset, 256), 256)
-            target[:, columns] = product_of(source, 256)
-
+            wide = jnp.concatenate([scale[...]] * 2, axis=1)
+            target[:, columns] = ((acc[:, source] + group_product(dz, source)) * wide).astype(BF)
+
+    def up_group(dz):
+        pump_all(lambda piece: piece[0] == "up" and dz_of(piece) == dz)
+
+    up_group(0)
+    up_group(1)
+    group_loop((0, 1), True, 0, 4)
+    pump_until(59.0)
+    group_loop((0, 1), True, 4, 8)
+    pump_until(62.0)
+    up_group(3)
+    group_loop((3,), False, 0, 4)
+    pump_until(66.0)
+    group_loop((3,), False, 4, 8)
+    pump_until(69.0)
+    up_group(2)
     now = max(action[0] for action in actions if action[1] == 0 and action[3][0] == "up")
-    pump_until(now + 1.0)
-    up_loop(gate, 0, 0, 2)
-    pump_until(now + 4.0)
-    up_loop(gate, 0, 2, 4)
+    final_loop(2, gate, 0)
+    tail = ((acc[:, LAST] + group_product(2, LAST)) * scale[...]).astype(BF).astype(F32)
+    gate_tail, value_tail = acc.at[:, 0:128], acc.at[:, 128:256]
+    gate_tail[...] = pltpu.roll(tail, 64, 1)
+    value_tail[...] = pltpu.roll(tail, 32, 1)
     edge_out[...] = gate[TOKENS - 16 :, :]
     edge_tail_out[...] = gate_tail[TOKENS - 16 :, :]
     launch(remote(edge_out, edge, edge_send.at[0], edge_recv.at[0], later(1)))
     launch(remote(edge_tail_out, edge_tail, edge_send.at[1], edge_recv.at[1], later(1)))
-    pump_until(now + 7.0)
-    up_loop(value, MAIN, 0, 2)
-    pump_until(now + 10.0)
-    up_loop(value, MAIN, 2, 4)
-    pump_until(now + 13.0)
-    remote(edge_out, edge, edge_send.at[0], edge_recv.at[0], sibling).wait_recv()
-    remote(edge_tail_out, edge_tail, edge_send.at[1], edge_recv.at[1], sibling).wait_recv()
-
+    pump_until(now + 2.0)
+    final_loop(2, value, MAIN)
+    pump_until(now + 4.0)
+
+    head = slice(0, 16)
     place = lax.broadcasted_iota(jnp.int32, (TOKENS, 1), 0)
     seg = columns_of[:, 0:1]
     last_one, second_one = carried["last"][:, 0:1], carried["second"][:, 0:1]
     before = jnp.where(place == 0, last_one, columns_of[:, 1:2])
     before_two = jnp.where(place == 0, second_one, jnp.where(place == 1, last_one, columns_of[:, 2:3]))
-    near_mask = jnp.where(before == seg, 1.0, 0.0)
-    far_mask = jnp.where(before_two == seg, 1.0, 0.0)
-    wide_near = jnp.broadcast_to(near_mask, (TOKENS, 128)) > 0.5
-    wide_far = jnp.broadcast_to(far_mask, (TOKENS, 128)) > 0.5
-    at_first = jnp.broadcast_to(place, (TOKENS, 128)) == 0
-    at_second = jnp.broadcast_to(place, (TOKENS, 128)) == 1
-
-    def mixed(g, v, tap, previous):
+    wide_near = jnp.broadcast_to(jnp.where(before == seg, 1.0, 0.0), (TOKENS, 128)) > 0.5
+    wide_far = jnp.broadcast_to(jnp.where(before_two == seg, 1.0, 0.0), (TOKENS, 128)) > 0.5
+    at_first = jnp.broadcast_to(place[head], (16, 128)) == 0
+    at_second = jnp.broadcast_to(place[head], (16, 128)) == 1
+
+    def gated(g, one, two, v, tap, near, far):
+        conv = tap[2:3, :] * g + tap[1:2, :] * jnp.where(near, one, 0.0) + tap[0:1, :] * jnp.where(far, two, 0.0)
+        return conv * jax.nn.sigmoid(conv) * v
+
+    def mixed(g, v, tap):
+        return gated(g, pltpu.roll(g, 1, 0), pltpu.roll(g, 2, 0), v, tap, wide_near, wide_far)
+
+    def mixed_head(g, v, tap, previous):
         one = jnp.where(at_first, previous[15:16, :], pltpu.roll(g, 1, 0))
         two = jnp.where(
             at_first, previous[14:15, :], jnp.where(at_second, previous[15:16, :], pltpu.roll(g, 2, 0))
         )
-        conv = (
-            tap[2:3, :] * g
-            + tap[1:2, :] * jnp.where(wide_near, one, 0.0)
-            + tap[0:1, :] * jnp.where(wide_far, two, 0.0)
-        )
-        return (conv * jax.nn.sigmoid(conv) * v).astype(BF)
+        return gated(g, one, two, v, tap, wide_near[head], wide_far[head])
 
     lanes = lax.broadcasted_iota(jnp.int32, (TOKENS, 128), 1)
     in_tail = (lanes >= 64) & (lanes < 96)
     tap_tail = jnp.concatenate([jnp.zeros((3, 64), F32), taps[:, MAIN:], jnp.zeros((3, 32), F32)], axis=1)
-    hidden_tail[...] = jnp.where(
-        in_tail, mixed(gate_tail[...], value_tail[...], tap_tail, edge_tail[...]).astype(F32), 0.0
-    ).astype(BF)
+    gate_head[...] = gate[head, :]
 
     def mix_loop():
         @pl.loop(0, MAIN // 128)
         def _(n):
             columns = pl.ds(pl.multiple_of(n * 128, 128), 128)
-            hidden[:, columns] = mixed(
-                gate[:, columns].astype(F32),
-                value[:, columns].astype(F32),
-                taps[:, columns],
-                edge[:, columns].astype(F32),
-            )
+            gate[:, columns] = mixed(
+                gate[:, columns].astype(F32), value[:, columns].astype(F32), taps[:, columns]
+            ).astype(BF)
 
     mix_loop()
-    pump_until(now + 15.5)
+    hidden_tail[...] = jnp.where(in_tail, mixed(gate_tail[...], value_tail[...], tap_tail), 0.0).astype(BF)
+    pump_until(now + 5.0)
+    remote(edge_out, edge, edge_send.at[0], edge_recv.at[0], sibling).wait_recv()
+    remote(edge_tail_out, edge_tail, edge_send.at[1], edge_recv.at[1], sibling).wait_recv()
+    hidden_tail[head, :] = jnp.where(
+        in_tail[head], mixed_head(gate_tail[head, :], value_tail[head, :], tap_tail, edge_tail[...]), 0.0
+    ).astype(BF)
+
+    @pl.loop(0, MAIN // 128)
+    def _(n):
+        columns = pl.ds(pl.multiple_of(n * 128, 128), 128)
+        gate[head, columns] = mixed_head(
+            gate_head[:, columns].astype(F32),
+            value[head, columns].astype(F32),
+            taps[:, columns],
+            edge[:, columns].astype(F32),
+        ).astype(BF)
+
+    pump_until(now + 6.0)
 
     def place_of(u):
         return slice(u * UNIT, (u + 1) * UNIT)
@@ -586,7 +628,7 @@
         main = jnp.concatenate([down[source, :] for source in sources], axis=0)
         rest = jnp.concatenate([up[source, 2 * MAIN :] for source in sources], axis=0)
         result = (
-            lax.dot_general(main, hidden[...], NT, preferred_element_type=F32)
+            lax.dot_general(main, gate[...], NT, preferred_element_type=F32)
             + lax.dot_general(rest, hidden_tail[...], NT, preferred_element_type=F32)
         ).astype(BF)
         for index, p in enumerate(ps):
@@ -605,7 +647,7 @@
         return remote(
             dshare.at[target, 1 - c, :, place_of(u), :],
             dsib.at[target, :, place_of(u), :],
-            dsib_send.at[k],
+            dsib_send.at[0],
             dsib_recv.at[k],
             sibling,
         )
@@ -621,7 +663,7 @@
             "r1": (prev_y, 1, dfar_r.at[1, rows_, :], down_y),
         }[kind]
         k = KINDS.index(kind)
-        return remote(dcomb.at[source, part, rows_, :], buffer, drs_send.at[k, u], drs_recv.at[k, u], device)
+        return remote(dcomb.at[source, part, rows_, :], buffer, drs_send.at[0], drs_recv.at[k, u], device)
 
     def down_combine(p):
         dz, colour, half_ = p
@@ -681,7 +723,7 @@
         completed.setdefault(dz_u, 0.0)
     order = sorted(completed, key=lambda p: (completed[p], p))
     groups = [order[k : k + 2] for k in range(0, 16, 2)]
-    start_time = now + 15.5
+    start_time = now + 7.0
     for index in range(len(groups) + RELAY_LAG):
         if index < len(groups):
             ps = groups[index]
@@ -694,8 +736,6 @@
         if index >= RELAY_LAG:
             for p in groups[index - RELAY_LAG]:
                 down_relay(p)
-        if index == len(groups):
-            drain(8)
     for kind in ("l1", "r0", "l0", "r1"):
         for u in range(4):
             dcopy(kind, u).wait_recv()
@@ -710,10 +750,21 @@
         stores.append(pltpu.make_async_copy(result.at[here, :], out.at[here, :], out_sem.at[i]))
         stores[i].start()
 
-    for kind in KINDS:
-        for u in range(4):
-            dcopy(kind, u).wait_send()
-    drain(0)
+    for ref, sem in (
+        (up.at[: 60 * UNIT], send_up),
+        (down.at[: 60 * UNIT], send_down),
+        (states, state_send),
+        (metas, meta_send),
+        (comb, sib_send),
+        (comb.at[:3], rs_send),
+        (comb.at[:3], ag_send),
+        (comb, pass_send),
+        (dsib, dsib_send),
+        (dcomb.at[:3], drs_send),
+    ):
+        sent(ref, sem)
+    remote(edge_out, edge, edge_send.at[0], edge_recv.at[0], sibling).wait_send()
+    remote(edge_tail_out, edge_tail, edge_send.at[1], edge_recv.at[1], sibling).wait_send()
     for store in stores:
         store.wait()
 
@@ -750,16 +801,15 @@
         pltpu.VMEM((TOKENS, OWN), BF),
         pltpu.VMEM((TOKENS, OWN), BF),
         pltpu.VMEM((TOKENS, OWN), F32),
+        pltpu.VMEM((TOKENS, 2 * MAIN + 128), F32),
         pltpu.VMEM((TOKENS, MAIN), BF),
-        pltpu.VMEM((TOKENS, MAIN), BF),
-        pltpu.VMEM((TOKENS, 128), F32),
-        pltpu.VMEM((TOKENS, 128), F32),
         pltpu.VMEM((TOKENS, MAIN), BF),
         pltpu.VMEM((TOKENS, 128), BF),
         pltpu.VMEM((16, MAIN), BF),
         pltpu.VMEM((16, 128), F32),
         pltpu.VMEM((16, MAIN), BF),
         pltpu.VMEM((16, 128), F32),
+        pltpu.VMEM((16, MAIN), BF),
         pltpu.VMEM((TOKENS, 128), F32),
         pltpu.VMEM((DH, HEADS), BF),
         pltpu.VMEM((8, HEADS), F32),
@@ -773,27 +823,27 @@
         pltpu.VMEM((2, ROWS, TOKENS), BF),
         pltpu.VMEM((2, ROWS, TOKENS), BF),
         dma((18,)),
+        dma((1,)),
         dma((64,)),
+        dma((1,)),
         dma((64,)),
-        dma((64,)),
-        dma((64,)),
+        dma((1,)),
         dma((4,)),
-        dma((4,)),
-        dma((4,)),
+        dma((1,)),
         dma((4,)),
         dma((2,)),
         dma((2,)),
+        dma((1,)),
         dma((CHUNKS,)),
-        dma((CHUNKS,)),
+        dma((1,)),
         dma((CHUNKS, 6)),
-        dma((CHUNKS, 6)),
+        dma((1,)),
         dma((CHUNKS, 4)),
-        dma((CHUNKS, 4)),
+        dma((1,)),
         dma((CHUNKS, 5)),
-        dma((CHUNKS, 5)),
+        dma((1,)),
         dma((16,)),
-        dma((16,)),
-        dma((6, 4)),
+        dma((1,)),
         dma((6, 4)),
         pltpu.VMEM((TOKENS, OWN), BF),
         dma((CHUNKS,)),
@@ -805,7 +855,7 @@
         out_shape=jax.ShapeDtypeStruct((TOKENS, OWN), BF),
         scratch_shapes=scratch,
         compiler_params=pltpu.CompilerParams(
-            collective_id=0, has_side_effects=True, vmem_limit_bytes=63000000
+            collective_id=0, has_side_effects=True, vmem_limit_bytes=67043328
         ),
         name="layer",
     )(

time: 142 us -> 137 us (0.965)
  Pallas kernels: 139 us -> 135 us
    pallas_call x1, Pallas kernels: 139 us -> 135 us  [body(): pl.pallas_call(layer_kernel, in_specs=[hbm] * 15, out_specs=hbm, out_shap...]
where the time goes in v3:
time: 137 us
  Pallas kernels  135 us (99%)
  local copies, waits for them, and re-layouts  1.94 us (1%)
    pallas_call x1, Pallas kernels, body(): pl.pallas_call(layer_kernel, in_specs=[hbm] * 15, out_specs=hbm, out_shap...  135 us

profile of v3, /device:TPU:16, one launch (start us, length us, event | category | flops | bytes accessed | tf_op | source)
XLA Modules:
  0.0 136.5 jit_solution(3737778273800727139)
XLA Ops:
  0.0 134.6 %layer.1 = bf16[768,384]{1,0:T(8,128)(2,1)} custom-call(bf16[768,384]{1,0:T(8,128)(2,1)} %resid_hbm.1, bf16[192,768]{1,0:T(8,128)(2,1)} %bitcast.9, bf16[192,768]{1,0:T(8,128)(2,1)} %bitcast.10, bf16[192,768]{1,0:T(8,128)(2,1)} %bitcast.11, bf16[192,768]{1,0:T(8,128)(2,1)} %bitcast.12, f32[2,768]{1,0:T(2,128)} %in_gate_hbm.1, f32[2,768]{1,0:T(2,128)} %forget_hbm.1, ...), custom_call_target="tpu_custom_call" | custom-call | tf_op jit(solution)/shard_map/layer/pallas_call | solution.py:851
  134.6 1.9 %copy.17 = bf16[768,384]{1,0:T(8,128)(2,1)} copy(bf16[768,384]{1,0:T(8,128)(2,1)} %layer.1) | data formatting | bytes 1179648

commit v4 on v3

--- a/solution.py
+++ b/solution.py
@@ -23,7 +23,7 @@
 UNIT = 48
 KINDS = ("near_l", "near_r", "l1", "r0", "l0", "r1")
 COMBINE_LAG = 1
-RELAY_LAG = 4
+RELAY_LAG = 7
 BF = jnp.bfloat16
 F32 = jnp.float32
 MESH = pl.DeviceIdType.MESH
@@ -31,11 +31,12 @@
 TN = (((0,), (0,)), ((), ()))
 
 RATES = {"up": 4.6, "down": 2.2}
-HOP = 4.0
-LEAD = 9.0
-LATE = (0, 1, 2, 4)
-LATE_ROW = ((3, 3, 3, 1), (1, 3, 6, 4))
-HELD = {("x", 1): 3.4, ("x", -1): 1.1, ("z", 1): 2.3, ("z", -1): 0.0}
+HOP = 3.0
+LEAD = 6.0
+IN_ORDER = True
+LATE = (2, 1, 2, 1)
+LATE_ROW = ((4, 3, 3, 1), (6, 0, 2, 4))
+HELD = {("x", 1): 2.6, ("x", -1): 0.9, ("z", 1): 1.8, ("z", -1): 0.0}
 EARLY = {0: 0, 1: 1, 3: 2, 2: 3}
 GROUP = 4 * ROWS
 
@@ -73,12 +74,13 @@
         return (0, EARLY[second if colour == 0 else first] - depth(start), half)
     row = second if colour == 0 else first
     row = row if half == 0 else -row % 4
-    return (1, LATE[colour * 2 + half] + LATE_ROW[colour][row] - 2 * depth(start) - (6 if second == 0 else 0))
+    return (1, LATE[colour * 2 + half] + LATE_ROW[colour][row] - 2 * depth(start) - (3 if second == 0 else 0))
 
 
 def gather_plan():
     ready = {link: [] for link in HELD}
     busy = dict(HELD)
+    issued = dict.fromkeys(HELD, 0.0)
     arrivals, actions, count, now = [], [], 0, 0.0
 
     def add(time, piece):
@@ -98,7 +100,8 @@
                 busy[link] = now + RATES[start[0][0]]
                 count += 1
                 heapq.heappush(arrivals, (busy[link] + HOP, count, landing(start)))
-                actions.append((max(since, now - LEAD), 1, count, start))
+                issued[link] = max(issued[link] if IN_ORDER else 0.0, since, now - LEAD)
+                actions.append((issued[link], 1, count, start))
         times = [busy[link] for link in ready if ready[link] and busy[link] > now] + [entry[0] for entry in arrivals[:1]]
         if not times:
             return sorted(actions, key=lambda action: action[:3])
@@ -265,7 +268,9 @@
         products.append(lax.dot_general(weighted, values[...], NT, preferred_element_type=F32))
         tops.append(top)
     total = [cumul[h : h + 1, TOKENS - 1 : TOKENS] for h in range(2)]
-    state_out[...] = (jnp.where(low, *products) * DH**-0.5).astype(BF)
+    state = jnp.where(low, *products) * DH**-0.5
+    state_out[:DH] = state[:, :128].astype(BF)
+    state_out[DH:] = jnp.concatenate([state[:UNIT, 128:], state[UNIT:, 128:]], axis=1).astype(BF)
     meta_out[...] = jnp.concatenate(
         [
             jnp.where(low, tops[0] + total[0], tops[1] + total[1]),
@@ -334,7 +339,9 @@
         state = jnp.zeros((DH, HEADS), F32)
         for by in range(1, 5):
             coef = jnp.where(logs[by - 1] > 0.5 * ABSENT, jnp.exp(logs[by - 1] - peak), 0.0)
-            state = state + coef * states[by - 1].astype(F32)
+            part = states[by - 1].astype(F32)
+            side = jnp.concatenate([part[DH:, :64], part[DH:, 64:]], axis=0)
+            state = state + coef * jnp.concatenate([part[:DH], side], axis=1)
         carried["state"] = jnp.concatenate(
             [jnp.where(low, state, 0.0), jnp.where(low, 0.0, state)], axis=0
         ).astype(BF)
@@ -722,7 +729,7 @@
     for dz_u in [(0, colour, half_) for colour in range(2) for half_ in range(2)]:
         completed.setdefault(dz_u, 0.0)
     order = sorted(completed, key=lambda p: (completed[p], p))
-    groups = [order[k : k + 2] for k in range(0, 16, 2)]
+    groups = [order[k : k + 2] for k in range(0, 12, 2)] + [[p] for p in order[12:]]
     start_time = now + 7.0
     for index in range(len(groups) + RELAY_LAG):
         if index < len(groups):
@@ -811,9 +818,9 @@
         pltpu.VMEM((16, 128), F32),
         pltpu.VMEM((16, MAIN), BF),
         pltpu.VMEM((TOKENS, 128), F32),
-        pltpu.VMEM((DH, HEADS), BF),
+        pltpu.VMEM((DH + UNIT, 128), BF),
         pltpu.VMEM((8, HEADS), F32),
-        pltpu.VMEM((4, DH, HEADS), BF),
+        pltpu.VMEM((4, DH + UNIT, 128), BF),
         pltpu.VMEM((4, 8, HEADS), F32),
         pltpu.VMEM((4, 2, 2, ROWS, TOKENS), BF),
         pltpu.VMEM((4, 2, ROWS, TOKENS), BF),

time: 137 us -> 132 us (0.964)
  Pallas kernels: 135 us -> 130 us
    pallas_call x1, Pallas kernels: 135 us -> 130 us  [body(): pl.pallas_call(layer_kernel, in_specs=[hbm] * 15, out_specs=hbm, out_shap...]
where the time goes in v4:
time: 132 us
  Pallas kernels  130 us (98%)
  local copies, waits for them, and re-layouts  1.94 us (1%)
    pallas_call x1, Pallas kernels, body(): pl.pallas_call(layer_kernel, in_specs=[hbm] * 15, out_specs=hbm, out_shap...  130 us

profile of v4, /device:TPU:16, one launch (start us, length us, event | category | flops | bytes accessed | tf_op | source)
XLA Modules:
  0.0 131.5 jit_solution(11300117702092200893)
XLA Ops:
  0.0 129.6 %layer.1 = bf16[768,384]{1,0:T(8,128)(2,1)} custom-call(bf16[768,384]{1,0:T(8,128)(2,1)} %resid_hbm.1, bf16[192,768]{1,0:T(8,128)(2,1)} %bitcast.9, bf16[192,768]{1,0:T(8,128)(2,1)} %bitcast.10, bf16[192,768]{1,0:T(8,128)(2,1)} %bitcast.11, bf16[192,768]{1,0:T(8,128)(2,1)} %bitcast.12, f32[2,768]{1,0:T(2,128)} %in_gate_hbm.1, f32[2,768]{1,0:T(2,128)} %forget_hbm.1, ...), custom_call_target="tpu_custom_call" | custom-call | tf_op jit(solution)/shard_map/layer/pallas_call | solution.py:858
  129.6 1.9 %copy.17 = bf16[768,384]{1,0:T(8,128)(2,1)} copy(bf16[768,384]{1,0:T(8,128)(2,1)} %layer.1) | data formatting | bytes 1179648

commit v5 on v4

--- a/solution.py
+++ b/solution.py
@@ -203,9 +203,23 @@
         row = (((z - dz + 4) % 4) * 4 + (x - dx + 4) % 4) * ROWS + colour * 96 + half * UNIT
         return pl.ds(pl.multiple_of(row, UNIT), UNIT)
 
+    slots = {"up": {}, "down": {}}
+    leaves = {}
+
+    def leaf_key(piece):
+        dz = dz_of(piece)
+        return ("up", dz) if piece[0] == "up" else ("down", (dz, piece[1], piece[2]))
+
     def slot(piece):
-        tensor, colour, half, first, second = piece
-        return ((colour * 2 + half) * 4 + first) * 4 + second
+        if follow(piece):
+            return slots[piece[0]][piece]
+        return slots[piece[0]][leaf_key(piece)]
+
+    def wait_leaves(key):
+        if key in leaves:
+            buffer, send, recv = gathered[key[0]]
+            place = buffer.at[: leaves[key] * UNIT, :]
+            remote(place, place, send.at[0], recv.at[slots[key[0]][key]], sibling).wait_recv()
 
     def begin(start):
         piece, axis, direction = start
@@ -216,7 +230,6 @@
 
     actions = gather_plan()
     position = [0]
-    arrived = set()
 
     def step():
         _, kind, _, item = actions[position[0]]
@@ -224,15 +237,25 @@
         if kind == 1:
             begin(item)
         else:
+            if not follow(item):
+                return
             buffer, send, recv = gathered[item[0]]
             place = buffer.at[origin(item), :]
             remote(place, place, send.at[0], recv.at[slot(item)], sibling).wait_recv()
-            arrived.add(item)
 
     middle = [0.0]
 
     def dz_of(piece):
         return piece[4] if piece[1] == 0 else piece[3]
+
+    for _, kind, _, item in actions:
+        if kind == 0:
+            table = slots[item[0]]
+            if follow(item):
+                table[item] = len(table)
+            else:
+                table.setdefault(leaf_key(item), len(table))
+                leaves[leaf_key(item)] = leaves.get(leaf_key(item), 0) + 1
 
     def pump_until(time):
         while position[0] < len(actions) and actions[position[0]][0] <= time:
@@ -536,6 +559,7 @@
 
     def up_group(dz):
         pump_all(lambda piece: piece[0] == "up" and dz_of(piece) == dz)
+        wait_leaves(("up", dz))
 
     up_group(0)
     up_group(1)
@@ -736,6 +760,8 @@
             ps = groups[index]
             pump_until(start_time + 2.0 * index)
             pump_all(lambda item: item[0] == "down" and piece_of(item) in ps)
+            for p in ps:
+                wait_leaves(("down", p))
             down_product(ps)
         if 0 <= index - COMBINE_LAG < len(groups):
             for p in groups[index - COMBINE_LAG]:
@@ -831,9 +857,9 @@
         pltpu.VMEM((2, ROWS, TOKENS), BF),
         dma((18,)),
         dma((1,)),
-        dma((64,)),
+        dma((32,)),
         dma((1,)),
-        dma((64,)),
+        dma((40,)),
         dma((1,)),
         dma((4,)),
         dma((1,)),

time: 132 us -> 132 us (level)
  no operation moved by 1% of the time
where the time goes in v5:
time: 132 us; the launch traced here: 131 us
  Pallas kernels  129 us (98%)
  local copies, waits for them, and re-layouts  1.94 us (1%)
    pallas_call x1, Pallas kernels, body(): pl.pallas_call(layer_kernel, in_specs=[hbm] * 15, out_specs=hbm, out_shap...  129 us

profile of v5, /device:TPU:16, one launch (start us, length us, event | category | flops | bytes accessed | tf_op | source)
XLA Modules:
  0.0 131.0 jit_solution(9911837099182678485)
XLA Ops:
  0.0 129.1 %layer.1 = bf16[768,384]{1,0:T(8,128)(2,1)} custom-call(bf16[768,384]{1,0:T(8,128)(2,1)} %resid_hbm.1, bf16[192,768]{1,0:T(8,128)(2,1)} %bitcast.9, bf16[192,768]{1,0:T(8,128)(2,1)} %bitcast.10, bf16[192,768]{1,0:T(8,128)(2,1)} %bitcast.11, bf16[192,768]{1,0:T(8,128)(2,1)} %bitcast.12, f32[2,768]{1,0:T(2,128)} %in_gate_hbm.1, f32[2,768]{1,0:T(2,128)} %forget_hbm.1, ...), custom_call_target="tpu_custom_call" | custom-call | tf_op jit(solution)/shard_map/layer/pallas_call | solution.py:884
  129.1 1.9 %copy.17 = bf16[768,384]{1,0:T(8,128)(2,1)} copy(bf16[768,384]{1,0:T(8,128)(2,1)} %layer.1) | data formatting | bytes 1179648
